TPU v7x, 256 devices: a whole 4x4x8 slice. The times are simulated.
256 devices in a mesh: ep: 128 (over z, y, x), tp: 2 (over core).
Axes of the slice: x: 4, y: 4, z: 8, core: 2. Of those that a mesh axis runs over, the one named last changes fastest.
Arguments:
- tokens: bfloat16 [2048, 2048], P('ep'), may hold values from -6 to 6
- lengths: int32 [2048], P('ep'), may hold values from 1024 to 8191
- prior_state: float32 [2048, 16, 64, 64], P('ep', 'tp'), may hold values from -2 to 2
- mix_gain: float32 [2048], replicated, may hold values from 0.1 to 1.9
- post_gain: float32 [2048], replicated, may hold values from 0.1 to 1.9
- ffn_gain: float32 [2048], replicated, may hold values from 0.1 to 1.9
- out_gain: float32 [2048], replicated, may hold values from 0.1 to 1.9
- query_weight: bfloat16 [2048, 1024], P('ep', 'tp'), may hold values from -0.125 to 0.125
- key_weight: bfloat16 [2048, 1024], P('ep', 'tp'), may hold values from -0.125 to 0.125
- value_weight: bfloat16 [2048, 1024], P('ep', 'tp'), may hold values from -0.125 to 0.125
- gate_weight: bfloat16 [2048, 1024], P('ep', 'tp'), may hold values from -0.125 to 0.125
- out_weight: bfloat16 [1024, 2048], P('tp', 'ep'), may hold values from -0.1875 to 0.1875
- routes: int32 [2048, 6], P('ep'), may hold values from 0 to 127, all different within a row; in each aligned block of 16 rows (0 to 15, 16 to 31, ...) at most 2 rows name the same one
- route_gates: float32 [2048, 6], P('ep'), may hold values from 0.1 to 0.9
- expert_gate: bfloat16 [128, 2048, 512], P('ep', None, 'tp'), may hold values from -0.125 to 0.125
- expert_up: bfloat16 [128, 2048, 512], P('ep', None, 'tp'), may hold values from -0.125 to 0.125
- expert_down: bfloat16 [128, 512, 2048], P('ep', 'tp'), may hold values from -0.25 to 0.25
- shared_gate: bfloat16 [2048, 512], P(None, 'tp'), may hold values from -0.125 to 0.125
- shared_up: bfloat16 [2048, 512], P(None, 'tp'), may hold values from -0.125 to 0.125
- shared_down: bfloat16 [512, 2048], P('tp'), may hold values from -0.25 to 0.25
Outputs:
- result: bfloat16 [2048, 2048], P('ep')
- new_state: float32 [2048, 16, 64, 64], P('ep', 'tp')
Inputs may be any that keep to these rules, and one draw needn't show every extreme that they name: `routes`: each row names 6 different experts. In the rows of one device (aligned blocks of 16 rows) no expert is named more than 2 times, and in every draw some expert is named exactly 2 times in some block.
All inputs are finite; a program needn't handle non-finite values.
Results may differ from a plain program's by a relative error of at most 0.02.
Values may be sent and summed in bfloat16 or wider, within the bound.
No kernel may reach another device: no remote copies, remote signals or barrier semaphores. Data moves between devices by JAX's collectives and lax.ppermute only.
A program may use at most 128 MiB of HBM per device.

v0:
```python
import jax
import jax.numpy as jnp
from jax import lax
from jax.sharding import Mesh
from jax.sharding import PartitionSpec as P

HEAD = 64
HEADS = 16
EP = ("ep_0", "ep_1", "ep_2")


EPS = 1e-06
THETA = 10000.0


def sent_together(arrays, axis, dim, along):
    widths = [a.shape[along] for a in arrays]
    both = jnp.concatenate(arrays, axis=along)
    out = lax.all_gather(both, axis, axis=dim, tiled=True)
    return tuple(jnp.split(out, [sum(widths[:k]) for k in range(1, len(widths))], axis=along))


def gathered_by_axis(value, axes, dim):
    for axis in reversed(axes):
        value = lax.all_gather(value, axis, axis=dim, tiled=True)
    return value


def sent_to_all(value, axis):
    copies = jnp.broadcast_to(value, (lax.axis_size(axis), *value.shape))
    return lax.all_to_all(copies, axis, split_axis=0, concat_axis=0, tiled=True)


def of_everyone(value, axis):
    return sent_to_all(value, axis).astype(jnp.float32).sum(axis=0)


def split_up(value, dim, count):
    before, after = (value.shape[:dim], value.shape[dim + 1 :])
    return jnp.moveaxis(value.reshape(*before, count, -1, *after), dim, 0)


def summed_on_arrival(value, axis, dim):
    count = lax.axis_size(axis)
    blocks = lax.all_to_all(split_up(value, dim, count), axis, 0, 0, tiled=True)
    return jnp.sum(blocks.astype(jnp.float32), axis=0)


def gathered_total(value, axis):
    blocks = lax.all_gather(value, axis)
    return blocks.sum(axis=0)


def in_order(blocks, dim):
    shape = list(blocks.shape[1:])
    shape[dim] *= blocks.shape[0]
    return jnp.moveaxis(blocks, 0, dim).reshape(shape)


def gathered_copies(value, axis, dim):
    blocks = sent_to_all(value, axis)
    return in_order(blocks, dim)


def rounded(values):
    return lax.optimization_barrier(values.astype(jnp.bfloat16)).astype(jnp.float32)


def scaled_rows(values, gain_row):
    widened = values.astype(jnp.float32)
    return widened * lax.rsqrt(jnp.mean(widened * widened, axis=-1, keepdims=True) + EPS) * gain_row


def rotate(vectors, lengths):
    half_dim = vectors.shape[-1] // 2
    frequency = THETA ** (-jnp.arange(half_dim, dtype=jnp.float32) / half_dim)
    angles = lengths.astype(jnp.float32)[:, None] * frequency[None, :]
    cosine = jnp.cos(angles)[:, None, :]
    sine_part = jnp.sin(angles)[:, None, :]
    leading = vectors[..., :half_dim]
    trailing = vectors[..., half_dim:]
    return jnp.concatenate(
        [leading * cosine - trailing * sine_part, trailing * cosine + leading * sine_part], axis=-1
    )


def decay_table(head_count):
    head_order = jnp.arange(head_count, dtype=jnp.float32)
    return 1.0 - jnp.exp2(-5.0 - 7.0 * head_order / (head_count - 1))


def retain(queries, keys_new, values, out_gate, prior_state, lengths, decays):
    seq_count = queries.shape[0]
    head_count = decays.shape[0]
    layout = (seq_count, head_count, HEAD)
    rot_query = rotate(queries.astype(jnp.float32).reshape(layout), lengths)
    rot_key = rotate(keys_new.astype(jnp.float32).reshape(layout), lengths) * HEAD ** (-0.5)
    wide_values = values.astype(jnp.float32).reshape(layout)
    from_state = jnp.einsum("shd,shde->she", rot_query, prior_state)
    self_term = jnp.sum(rot_query * rot_key, axis=-1, keepdims=True)
    read_out = decays[None, :, None] * from_state + self_term * wide_values
    new_state = (
        decays[None, :, None, None] * prior_state
        + rot_key[..., :, None] * wide_values[..., None, :]
    )
    normed = read_out * lax.rsqrt(jnp.mean(read_out * read_out, axis=-1, keepdims=True) + EPS)
    gated_rows = normed.reshape(seq_count, head_count * HEAD) * jax.nn.silu(
        out_gate.astype(jnp.float32)
    )
    return (gated_rows.astype(jnp.bfloat16), new_state)


def on_device(
    tokens,
    lengths,
    prior_state,
    mix_gain,
    post_gain,
    ffn_gain,
    out_gain,
    query_weight,
    key_weight,
    value_weight,
    gate_weight,
    out_weight,
    routes,
    route_gates,
    expert_gate,
    expert_up,
    expert_down,
    shared_gate,
    shared_up,
    shared_down,
):
    seq_here = tokens.shape[0]
    model_width = tokens.shape[1]
    local_cols = query_weight.shape[1]
    normed = scaled_rows(tokens, mix_gain).astype(jnp.bfloat16)
    pieces = sent_together((query_weight, key_weight, value_weight, gate_weight), EP, 0, 1)
    projected = tuple(
        (jnp.dot(normed, portion, preferred_element_type=jnp.float32) for portion in pieces)
    )
    queries, keys_new, values, out_gate = tuple(
        (member.astype(jnp.bfloat16) for member in projected)
    )
    heads_here = local_cols // HEAD
    decays = lax.dynamic_slice_in_dim(
        decay_table(HEADS), lax.axis_index("tp") * heads_here, heads_here, 0
    )
    retained, new_state = retain(queries, keys_new, values, out_gate, prior_state, lengths, decays)
    partial_mix = jnp.dot(
        retained, gathered_by_axis(out_weight, EP, 1), preferred_element_type=jnp.float32
    )
    mixed_sum = rounded(
        of_everyone(rounded(partial_mix).astype(jnp.bfloat16), "tp").astype(jnp.float32)
    )
    middle = rounded(tokens.astype(jnp.float32) + scaled_rows(mixed_sum, post_gain))
    moe_in = scaled_rows(middle, ffn_gain).astype(jnp.bfloat16)
    experts_all = lax.axis_size(EP)
    topk_here = routes.shape[1]
    capacity = seq_here * topk_here // experts_all + 2
    slot_count = experts_all * capacity
    flat_routes = routes.reshape(-1)
    onehot = (flat_routes[:, None] == jnp.arange(experts_all, dtype=jnp.int32)[None, :]).astype(
        jnp.int32
    )
    earlier = jnp.cumsum(onehot, axis=0) - onehot
    ranks = jnp.sum(earlier * onehot, axis=1)
    slot_ids = flat_routes * capacity + ranks
    placing = (jnp.arange(slot_count, dtype=jnp.int32)[:, None] == slot_ids[None, :]).reshape(
        slot_count, seq_here, topk_here
    )
    dispatch_rows = jnp.any(placing, axis=2).astype(jnp.bfloat16)
    combine = jnp.sum(
        jnp.where(placing, route_gates[None, :, :], jnp.zeros((), jnp.float32)), axis=2
    ).T
    outgoing = jnp.dot(dispatch_rows, moe_in, preferred_element_type=jnp.float32).astype(
        jnp.bfloat16
    )
    outgoing = outgoing.reshape(experts_all, capacity, model_width)
    gate_local = expert_gate[0]
    up_local = expert_up[0]
    down_local = expert_down[0]
    arrived = lax.all_to_all(outgoing, EP, split_axis=0, concat_axis=0, tiled=True)
    sources = arrived.shape[0]
    held_slots = arrived.shape[1]
    flat_in = arrived.reshape(sources * held_slots, model_width)
    hidden = (
        jax.nn.silu(jnp.dot(flat_in, gate_local, preferred_element_type=jnp.float32))
        * jnp.dot(flat_in, up_local, preferred_element_type=jnp.float32)
    ).astype(jnp.bfloat16)
    partial_out = rounded(jnp.dot(hidden, down_local, preferred_element_type=jnp.float32))
    expert_sum = summed_on_arrival(partial_out.astype(jnp.bfloat16), "tp", 1).astype(jnp.bfloat16)
    returned = lax.all_to_all(
        expert_sum.reshape(sources, held_slots, -1), EP, split_axis=0, concat_axis=0, tiled=True
    )
    back_rows = returned.reshape(slot_count, -1).astype(jnp.float32)
    routed = jnp.dot(combine, back_rows)
    shared_hidden = (
        jax.nn.silu(jnp.dot(moe_in, shared_gate, preferred_element_type=jnp.float32))
        * jnp.dot(moe_in, shared_up, preferred_element_type=jnp.float32)
    ).astype(jnp.bfloat16)
    shared_part = rounded(jnp.dot(shared_hidden, shared_down, preferred_element_type=jnp.float32))
    shared_out = summed_on_arrival(shared_part.astype(jnp.bfloat16), "tp", 1).astype(jnp.bfloat16)
    mixture = shared_out.astype(jnp.float32) + routed
    squares = gathered_total(jnp.sum(mixture * mixture, axis=1, keepdims=True), "tp")
    half_cols = mixture.shape[1]
    offset = lax.axis_index("tp") * half_cols
    gain_part = lax.dynamic_slice_in_dim(out_gain, offset, half_cols, 0)
    middle_part = lax.dynamic_slice_in_dim(middle, offset, half_cols, 1)
    scale_rows = lax.rsqrt(squares / model_width + EPS)
    half_result = (middle_part + mixture * scale_rows * gain_part).astype(jnp.bfloat16)
    result = gathered_copies(half_result, "tp", 1)
    return (result, new_state)


def solution(mesh):
    finer = Mesh(mesh.devices.reshape(8, 4, 4, mesh.shape["tp"]), ("ep_0", "ep_1", "ep_2", "tp"))
    in_specs = (
        P(EP, None),
        P(EP),
        P(EP, "tp", None, None),
        P(),
        P(),
        P(),
        P(),
        P(EP, "tp"),
        P(EP, "tp"),
        P(EP, "tp"),
        P(EP, "tp"),
        P("tp", EP),
        P(EP, None),
        P(EP, None),
        P(EP, None, "tp"),
        P(EP, None, "tp"),
        P(EP, "tp", None),
        P(None, "tp"),
        P(None, "tp"),
        P("tp", None),
    )
    out_specs = (P(EP, None), P(EP, "tp", None, None))
    return jax.shard_map(
        on_device, mesh=finer, in_specs=in_specs, out_specs=out_specs, check_vma=False
    )
```

profile of v0, /device:TPU:1, one launch (start us, length us, event | category | flops | bytes accessed | tf_op | source)
XLA Modules:
  0.0 289.7 jit_solution(9632476741348007114)
XLA Ops:
  7.3 1.5 pad_maximum_fusion
  8.8 0.0 all-gather.6.cloned.1.call-start
  8.8 10.4 %all_gather.16 = bf16[512,64]{0,1:T(8,128)(2,1)S(1)} all-gather(bf16[512,16]{0,1:T(8,128)(2,1)} %param.31), channel_id=1, replica_groups=mesh['ep_0'=8,'ep_1'=4,'ep_2'=4,'tp'=2] {'ep_2'}, dimensions={1}, use_global_device_ids=true | all-gather | bytes 81920 | tf_op jit(solution)/shard_map/all_gather | solution.py:25
  19.2 10.6 %all_gather.17 = bf16[512,256]{0,1:T(8,128)(2,1)} all-gather(bf16[512,64]{0,1:T(8,128)(2,1)S(1)} %all_gather.16), channel_id=1, replica_groups=mesh['ep_0'=8,'ep_1'=4,'ep_2'=4,'tp'=2] {'ep_1'}, dimensions={1}, use_global_device_ids=true | all-gather | bytes 327680 | tf_op jit(solution)/shard_map/all_gather | solution.py:25
  29.8 0.7 convert_element_type.88
  30.5 0.8 copy.46
  31.2 0.1 eq.30
  31.3 0.1 fusion.55
  31.4 0.1 reduce_window_sum.11
  31.5 0.2 select_reduce_fusion.1
  31.7 0.1 reduce_sum.127
  31.8 0.1 copy.47
  31.9 0.1 dynamic_slice.9
  32.0 0.7 multiply_add_fusion.3
  32.7 0.1 fusion.54
  32.8 1.0 fusion.49
  33.8 0.1 multiply_cosine_fusion
  33.9 102.7 %all-gather.4.cloned.1.call-done = bf16[2048,2048]{1,0:T(8,128)(2,1)} async-done(((bf16[16,2048]{1,0:T(8,128)(2,1)}), bf16[2048,2048]{1,0:T(8,128)(2,1)}) %all-gather.4.cloned.1.call-update) | async-done | bytes 8388624 | tf_op jit(solution)/shard_map/all_gather | solution.py:19
  136.6 2.1 fusion.15
  138.7 0.1 reshape.196
  138.7 2.1 fusion.21
  140.8 0.1 reshape.198
  140.9 2.0 fusion.27
  142.9 0.1 reshape.200
  143.0 0.1 multiply_subtract_fusion
  143.1 0.1 pad_maximum_fusion.1
  143.2 2.8 fusion.77
  146.1 0.2 multiply_reduce_fusion.2
  146.3 0.1 broadcast_multiply_fusion
  146.4 0.1 reshape.187
  146.5 29.0 %all-gather.6.cloned.1.call-done = bf16[512,2048]{0,1:T(8,128)(2,1)} async-done(((bf16[512,256]{0,1:T(8,128)(2,1)}), bf16[512,2048]{0,1:T(8,128)(2,1)}) %all-gather.6.cloned.1.call-update) | async-done | bytes 2097168 | tf_op jit(solution)/shard_map/all_gather | solution.py:25
  175.5 3.3 %convolution_convert_fusion.3 = bf16[16,2048]{1,0:T(8,128)(2,1)S(1)} fusion(bf16[512,2048]{0,1:T(8,128)(2,1)} %all-gather.6.cloned.1.call-done, f32[16,512]{1,0:T(8,128)S(1)} %reshape.187, bf16[2048,2048]{1,0:T(8,128)(2,1)} %all-gather.4.cloned.1.call-done, bf16[16,2048]{1,0:T(8,128)(2,1)S(1)} %copy-done.2, f32[2048]{0:T(1024)S(1)} %copy-done.4, ...), kind=kOutput, calls=%fused_computation.5 | convolution fusion | flops 67338240 | bytes 4366400 | tf_op jit(solution)/shard_map/dot_general | solution.py:151
  178.8 8.5 %all_to_all.30 = bf16[2,16,2048]{2,1,0:T(8,128)(2,1)S(1)} all-to-all(bf16[2,16,2048]{2,1,0:T(8,128)(2,1)S(1)} %broadcast_in_dim.12), channel_id=1, replica_groups=mesh['ep_0'=8,'ep_1'=4,'ep_2'=4,'tp'=2] {'tp'}, dimensions={0} | all-to-all | bytes 262144 | tf_op jit(solution)/shard_map/all_to_all | solution.py:31
  187.3 0.1 fusion.47
  187.4 0.1 fusion.52
  187.5 0.1 multiply_reduce_fusion
  187.7 0.5 convolution_convert_fusion
  188.1 1.5 reshape.189
  189.6 11.1 %all-to-all-start.2 = ((bf16[128,2,2048]{2,1,0:T(2,128)(2,1)}), bf16[128,2,2048]{2,1,0:T(2,128)(2,1)S(1)}, u32[]{:S(2)}, u32[]{:S(2)}) async-start(bf16[128,2,2048]{2,1,0:T(2,128)(2,1)} %reshape.189), calls=%async_computation.2 | async-start | bytes 2097152 | tf_op jit(solution)/shard_map/all_to_all | solution.py:184
  200.7 1.5 fusion.71
  202.3 2.0 convolution_convert_fusion.2
  204.3 0.7 copy.58
  204.9 25.0 %all-to-all-done.2 = bf16[128,2,2048]{2,1,0:T(2,128)(2,1)S(1)} async-done(((bf16[128,2,2048]{2,1,0:T(2,128)(2,1)}), bf16[128,2,2048]{2,1,0:T(2,128)(2,1)S(1)}, u32[]{:S(2)}, u32[]{:S(2)}) %all-to-all-start.2) | async-done | bytes 1048608 | tf_op jit(solution)/shard_map/all_to_all | solution.py:184
  229.9 0.4 reshape.190
  230.3 2.4 fusion.40
  232.7 2.5 convolution_convert_fusion.1
  235.3 0.1 copy.57
  235.3 7.3 %all_to_all.31 = bf16[2,256,1024]{2,1,0:T(8,128)(2,1)S(1)} all-to-all(bf16[2,256,1024]{2,1,0:T(8,128)(2,1)S(1)} %bitcast.44), channel_id=1, replica_groups=mesh['ep_0'=8,'ep_1'=4,'ep_2'=4,'tp'=2] {'tp'}, dimensions={0} | all-to-all | bytes 2097152 | tf_op jit(solution)/shard_map/all_to_all | solution.py:45
  242.6 3.7 %all-to-all-start.1 = ((bf16[2,16,1024]{2,1,0:T(8,128)(2,1)}), bf16[2,16,1024]{2,1,0:T(8,128)(2,1)S(1)}, u32[]{:S(2)}, u32[]{:S(2)}) async-start(bf16[2,16,1024]{2,1,0:T(8,128)(2,1)} %bitcast.43), calls=%async_computation.1 | async-start | bytes 131072 | tf_op jit(solution)/shard_map/all_to_all | solution.py:45
  246.3 0.2 reduce_sum.129
  246.5 1.0 reshape.192
  247.5 6.2 %all-to-all-start.4 = ((bf16[128,2,1024]{2,1,0:T(2,128)(2,1)}), bf16[128,2,1024]{2,1,0:T(2,128)(2,1)S(1)}, u32[]{:S(2)}, u32[]{:S(2)}) async-start(bf16[128,2,1024]{2,1,0:T(2,128)(2,1)} %reshape.192), calls=%async_computation.4 | async-start | bytes 1048576 | tf_op jit(solution)/shard_map/all_to_all | solution.py:194
  253.7 0.6 dynamic-slice
  255.0 0.1 select_reduce_fusion
  255.1 4.3 %multiply_add_fusion = f32[16,8,64,64]{3,2,1,0:T(8,128)} fusion(f32[16,8,64,64]{3,2,1,0:T(8,128)} %param.22, f32[16,8,64]{2,1,0:T(8,128)S(1)} %reshape.200, f32[16,8,64]{2,1,0:T(8,128)S(1)} %get-tuple-element.15, f32[8]{0:T(128)S(1)} %dynamic_slice.9), kind=kLoop, calls=%fused_computation.1 | loop fusion | flops 1572864 | bytes 4259872 | tf_op jit(solution)/shard_map/add | solution.py:103
  259.4 13.7 %all-to-all-done.4 = bf16[128,2,1024]{2,1,0:T(2,128)(2,1)S(1)} async-done(((bf16[128,2,1024]{2,1,0:T(2,128)(2,1)}), bf16[128,2,1024]{2,1,0:T(2,128)(2,1)S(1)}, u32[]{:S(2)}, u32[]{:S(2)}) %all-to-all-start.4) | async-done | bytes 524320 | tf_op jit(solution)/shard_map/all_to_all | solution.py:194
  273.1 0.2 reshape.193
  273.3 0.3 multiply_reduce_fusion.1
  273.6 0.2 dynamic-update-slice
  273.8 4.4 %all-reduce = f32[32]{0:T(128)S(1)} all-reduce(f32[32]{0:T(128)S(1)} %dynamic-update-slice), channel_id=2, replica_groups=mesh['ep_0'=8,'ep_1'=4,'ep_2'=4,'tp'=2] {'tp'}, use_global_device_ids=true, to_apply=%add | all-reduce | flops 32 | bytes 256
  278.2 0.1 reshape.201
  278.3 0.1 add_convert_fusion
  278.4 3.8 %all_to_all.32 = bf16[2,16,1024]{2,1,0:T(8,128)(2,1)S(1)} all-to-all(bf16[2,16,1024]{2,1,0:T(8,128)(2,1)S(1)} %broadcast_in_dim.15), channel_id=1, replica_groups=mesh['ep_0'=8,'ep_1'=4,'ep_2'=4,'tp'=2] {'tp'}, dimensions={0} | all-to-all | bytes 131072 | tf_op jit(solution)/shard_map/all_to_all | solution.py:31
  282.2 0.6 copy.54
  (36 shorter events, 0.3 us)
Async XLA Ops:
  7.2 225.5 %copy-start = (bf16[1,256,2048]{2,1,0:T(8,128)(2,1)S(1)}, bf16[1,256,2048]{2,1,0:T(8,128)(2,1)}, u32[]{:S(2)}) copy-start(bf16[1,256,2048]{2,1,0:T(8,128)(2,1)} %param.36) | copy-start | bytes 3145732
  7.2 133.7 %copy-start.2 = (bf16[16,2048]{1,0:T(8,128)(2,1)S(1)}, bf16[16,2048]{1,0:T(8,128)(2,1)}, u32[]{:S(2)}) copy-start(bf16[16,2048]{1,0:T(8,128)(2,1)} %param.20) | copy-start | bytes 196612
  7.2 133.7 %copy-start.4 = (f32[2048]{0:T(1024)S(1)}, f32[2048]{0:T(1024)}, u32[]{:S(2)}) copy-start(f32[2048]{0:T(1024)} %param.23) | copy-start | bytes 24580
  7.2 129.4 %all-gather.4.cloned.1.call-start = ((), (), s32[]{:S(2)}) async-start(), calls=%async_computation.6 | async-start | bytes 8454144 | tf_op jit(solution)/shard_map/all_gather | solution.py:19
  8.8 166.7 %all-gather.6.cloned.1.call-start = ((), (), s32[]{:S(2)}) async-start(), calls=%async_computation.7 | async-start | bytes 2359296 | tf_op jit(solution)/shard_map/all_gather | solution.py:25
  143.2 44.2 %copy-start.5 = (f32[2048]{0:T(1024)S(1)}, f32[2048]{0:T(1024)}, u32[]{:S(2)}) copy-start(f32[2048]{0:T(1024)} %param.24) | copy-start | bytes 24580
  143.2 44.4 %copy-start.3 = (f32[2048]{0:T(1024)S(1)}, f32[2048]{0:T(1024)}, u32[]{:S(2)}) copy-start(f32[2048]{0:T(1024)} %param.25) | copy-start | bytes 24580
  178.7 23.5 %copy-start.1 = (bf16[256,2048]{1,0:T(8,128)(2,1)S(1)}, bf16[256,2048]{1,0:T(8,128)(2,1)}, u32[]{:S(2)}) copy-start(bf16[256,2048]{1,0:T(8,128)(2,1)} %param.39) | copy-start | bytes 3145732
  189.6 40.2 %all-to-all-start.2 = ((bf16[128,2,2048]{2,1,0:T(2,128)(2,1)}), bf16[128,2,2048]{2,1,0:T(2,128)(2,1)S(1)}, u32[]{:S(2)}, u32[]{:S(2)}) async-start(bf16[128,2,2048]{2,1,0:T(2,128)(2,1)} %reshape.189), calls=%async_computation.2 | async-start | bytes 2097152 | tf_op jit(solution)/shard_map/all_to_all | solution.py:184
  235.2 18.5 %copy-start.7 = (u32[256]{0:T(256)S(1)}, u32[256]{0:T(256)}, u32[]{:S(2)}) copy-start(u32[256]{0:T(256)} %constant.79) | copy-start | bytes 3076
  235.3 19.7 %copy-start.6 = (f32[16,6]{0,1:T(8,128)S(1)}, f32[16,6]{0,1:T(8,128)}, u32[]{:S(2)}) copy-start(f32[16,6]{0,1:T(8,128)} %param.33) | copy-start | bytes 1156
  242.6 4.9 %all-to-all-start.1 = ((bf16[2,16,1024]{2,1,0:T(8,128)(2,1)}), bf16[2,16,1024]{2,1,0:T(8,128)(2,1)S(1)}, u32[]{:S(2)}, u32[]{:S(2)}) async-start(bf16[2,16,1024]{2,1,0:T(8,128)(2,1)} %bitcast.43), calls=%async_computation.1 | async-start | bytes 131072 | tf_op jit(solution)/shard_map/all_to_all | solution.py:45
  247.5 25.6 %all-to-all-start.4 = ((bf16[128,2,1024]{2,1,0:T(2,128)(2,1)}), bf16[128,2,1024]{2,1,0:T(2,128)(2,1)S(1)}, u32[]{:S(2)}, u32[]{:S(2)}) async-start(bf16[128,2,1024]{2,1,0:T(2,128)(2,1)} %reshape.192), calls=%async_computation.4 | async-start | bytes 1048576 | tf_op jit(solution)/shard_map/all_to_all | solution.py:194
  255.1 23.2 %dynamic-slice-start = ((f32[2048]{0:T(1024)}, s32[]{:T(128)}), f32[1024]{0:T(1024)S(1)}, s32[]{:S(2)}) async-start(f32[2048]{0:T(1024)} %param.26, s32[]{:T(128)} %select_n.12), calls=%async_computation.8 | async-start | bytes 8704 | tf_op jit(solution)/shard_map/dynamic_slice | solution.py:209
Sparse Core Ops, SparseCore 0:
  12.2 124.3 all-gather.3
  138.4 37.0 all-gather.5
where the time goes:
time: 291 us; the launch traced here: 290 us
  waiting for transfers between devices  170 us (58%)
  blocking collectives  44.9 us (15%)
  matrix products  21.4 us (7%)
  starting transfers between devices  21 us (7%)
  between operations  15 us (5%)
  other arithmetic  10.1 us (3%)
  local copies, waits for them, and re-layouts  6.89 us (2%)
    all_gather x1, waiting for transfers between devices, sent_together(): out = lax.all_gather(both, axis, axis=dim, tiled=True)  103 us
    all_gather x1, waiting for transfers between devices, gathered_by_axis(): value = lax.all_gather(value, axis, axis=dim, tiled=True)  29 us
    all_to_all x1, waiting for transfers between devices, on_device(): lax.all_to_all(outgoing, EP, split_axis=0, concat_axis=0, tiled=True)  25 us
    all_gather x2, blocking collectives, gathered_by_axis(): value = lax.all_gather(value, axis, axis=dim, tiled=True)  21 us
    all_to_all x1, waiting for transfers between devices, on_device(): lax.all_to_all(expert_sum.reshape(sources, held_slots, -1), EP, split_axi...  13.7 us
    all_to_all x2, blocking collectives, sent_to_all(): return lax.all_to_all(copies, axis, split_axis=0, concat_axis=0, tiled=True)  12.3 us
    all_to_all x1, starting transfers between devices, on_device(): lax.all_to_all(outgoing, EP, split_axis=0, concat_axis=0, tiled=True)  11.1 us
    all_to_all x1, blocking collectives, summed_on_arrival(): blocks = lax.all_to_all(split_up(value, dim, count), axis, 0, 0, tiled=True)  7.25 us
  transfers between devices with their start and end apart: 5, of which 4 were waited for; matrix products, arithmetic and copies ran while one was open for 8% of the time, Pallas kernels for 0%

commit v1 on v0

v1 whole, which is shorter than its diff:
```python
import jax
import jax.numpy as jnp
from jax import lax
from jax.sharding import Mesh
from jax.sharding import PartitionSpec as P

HEAD = 64
HEADS = 16
Z, Y, X = "ep_0", "ep_1", "ep_2"
EP = (Z, Y, X)


EPS = 1e-06
THETA = 10000.0


def exchanged(blocks, axes):
    return lax.all_to_all(blocks, axes, split_axis=0, concat_axis=0, tiled=True)


def copies(value, count):
    return jnp.broadcast_to(value, (count, *value.shape))


def from_partner(value):
    return lax.ppermute(value, "tp", [(0, 1), (1, 0)])


def gathered_ahead(value, axis):
    size = lax.axis_size(axis)
    others = [
        lax.ppermute(value, axis, [((i + j) % size, i) for i in range(size)])
        for j in range(1, size)
    ]
    return jnp.stack([value, *others])


def rolled_lanes(rows, start):
    doubled = jnp.concatenate([rows, rows], axis=1)
    return lax.dynamic_slice_in_dim(doubled, start, rows.shape[1], 1)


def rounded(values):
    return lax.optimization_barrier(values.astype(jnp.bfloat16)).astype(jnp.float32)


def scaled_rows(values, gain_row):
    widened = values.astype(jnp.float32)
    return widened * lax.rsqrt(jnp.mean(widened * widened, axis=-1, keepdims=True) + EPS) * gain_row


def rotate(vectors, lengths):
    half_dim = vectors.shape[-1] // 2
    frequency = THETA ** (-jnp.arange(half_dim, dtype=jnp.float32) / half_dim)
    angles = lengths.astype(jnp.float32)[:, None] * frequency[None, :]
    cosine = jnp.cos(angles)[:, None, :]
    sine_part = jnp.sin(angles)[:, None, :]
    leading = vectors[..., :half_dim]
    trailing = vectors[..., half_dim:]
    return jnp.concatenate(
        [leading * cosine - trailing * sine_part, trailing * cosine + leading * sine_part], axis=-1
    )


def decay_table(head_count):
    head_order = jnp.arange(head_count, dtype=jnp.float32)
    return 1.0 - jnp.exp2(-5.0 - 7.0 * head_order / (head_count - 1))


def retain(queries, keys_new, values, out_gate, prior_state, lengths, decays):
    seq_count = queries.shape[0]
    head_count = decays.shape[0]
    layout = (seq_count, head_count, HEAD)
    rot_query = rotate(queries.astype(jnp.float32).reshape(layout), lengths)
    rot_key = rotate(keys_new.astype(jnp.float32).reshape(layout), lengths) * HEAD ** (-0.5)
    wide_values = values.astype(jnp.float32).reshape(layout)
    from_state = jnp.einsum("shd,shde->she", rot_query, prior_state)
    self_term = jnp.sum(rot_query * rot_key, axis=-1, keepdims=True)
    read_out = decays[None, :, None] * from_state + self_term * wide_values
    new_state = (
        decays[None, :, None, None] * prior_state
        + rot_key[..., :, None] * wide_values[..., None, :]
    )
    normed = read_out * lax.rsqrt(jnp.mean(read_out * read_out, axis=-1, keepdims=True) + EPS)
    gated_rows = normed.reshape(seq_count, head_count * HEAD) * jax.nn.silu(
        out_gate.astype(jnp.float32)
    )
    return (gated_rows.astype(jnp.bfloat16), new_state)


def on_device(
    tokens,
    lengths,
    prior_state,
    mix_gain,
    post_gain,
    ffn_gain,
    out_gain,
    query_weight,
    key_weight,
    value_weight,
    gate_weight,
    out_weight,
    routes,
    route_gates,
    expert_gate,
    expert_up,
    expert_down,
    shared_gate,
    shared_up,
    shared_down,
):
    seq_here, width = tokens.shape
    cols = query_weight.shape[1]
    depth, rows_y, rows_x = (lax.axis_size(axis) for axis in EP)
    experts_all = depth * rows_y * rows_x
    plane = rows_y * rows_x
    mine_z = lax.axis_index(Z)
    core = lax.axis_index("tp")
    slab = width // depth
    half = width // 2

    kinds = jnp.stack([query_weight, key_weight, value_weight, gate_weight])
    my_kind = exchanged(kinds, X)
    wout_rows = out_weight.T
    shard = jnp.concatenate([my_kind.reshape(-1, cols), wout_rows], axis=0)
    ahead = gathered_ahead(shard, Z)
    kind_rows = my_kind.shape[0] * my_kind.shape[1]
    kind_weight = ahead[:, :kind_rows].reshape(-1, cols)
    wout_z = ahead[:, kind_rows:]

    normed = scaled_rows(tokens, mix_gain).astype(jnp.bfloat16)
    turned = rolled_lanes(normed, mine_z * slab)
    by_y = turned.reshape(seq_here, depth, rows_y, -1).transpose(2, 0, 1, 3)
    by_y = by_y.reshape(rows_y, 1, seq_here, width // rows_y)
    outgoing_rows = jnp.broadcast_to(by_y, (rows_y, rows_x, seq_here, width // rows_y))
    plane_rows = exchanged(outgoing_rows.reshape(plane, seq_here, -1), (Y, X))
    projected = jnp.dot(
        plane_rows.reshape(plane * seq_here, -1), kind_weight, preferred_element_type=jnp.float32
    ).astype(jnp.bfloat16)
    parts = exchanged(projected.reshape(plane, seq_here, cols), (Y, X))
    parts = parts.reshape(rows_y, rows_x, seq_here, cols).astype(jnp.float32)
    queries, keys_new, values, out_gate = jnp.sum(parts, axis=0).astype(jnp.bfloat16)

    heads_here = cols // HEAD
    decays = lax.dynamic_slice_in_dim(decay_table(HEADS), core * heads_here, heads_here, 0)
    retained, new_state = retain(queries, keys_new, values, out_gate, prior_state, lengths, decays)

    wout_zx = exchanged(copies(wout_z.reshape(-1, cols), rows_x), X)
    wout_zx = wout_zx.reshape(rows_x, depth, -1, cols).transpose(1, 0, 2, 3).reshape(-1, cols)
    retained_y = exchanged(copies(retained, rows_y), Y).reshape(rows_y * seq_here, cols)
    partial_mix = lax.dot_general(
        retained_y, wout_zx, (((1,), (1,)), ((), ())), preferred_element_type=jnp.float32
    ).astype(jnp.bfloat16)
    to_both = partial_mix.reshape(rows_y, 1, seq_here, -1)
    to_both = jnp.broadcast_to(to_both, (rows_y, 2, *to_both.shape[2:]))
    halves = exchanged(to_both.reshape(2 * rows_y, seq_here, -1), (Y, "tp"))
    halves = halves.reshape(rows_y, 2, seq_here, depth, -1).astype(jnp.float32)
    mixed = jnp.sum(halves, axis=1).astype(jnp.bfloat16)
    mixed = mixed.transpose(1, 2, 0, 3).reshape(seq_here, width)
    mixed_sum = rounded(rolled_lanes(mixed, (depth - mine_z) * slab))
    middle = rounded(tokens.astype(jnp.float32) + scaled_rows(mixed_sum, post_gain))
    moe_in = scaled_rows(middle, ffn_gain).astype(jnp.bfloat16)

    topk_here = routes.shape[1]
    capacity = seq_here * topk_here // experts_all + 2
    slot_count = experts_all * capacity
    flat_routes = routes.reshape(-1)
    onehot = (flat_routes[:, None] == jnp.arange(experts_all, dtype=jnp.int32)[None, :]).astype(
        jnp.int32
    )
    earlier = jnp.cumsum(onehot, axis=0) - onehot
    ranks = jnp.sum(earlier * onehot, axis=1)
    slot_ids = flat_routes * capacity + ranks
    placing = (jnp.arange(slot_count, dtype=jnp.int32)[:, None] == slot_ids[None, :]).reshape(
        slot_count, seq_here, topk_here
    )
    dispatch_rows = jnp.any(placing, axis=2).astype(jnp.bfloat16)
    combine = jnp.sum(
        jnp.where(placing, route_gates[None, :, :], jnp.zeros((), jnp.float32)), axis=2
    ).T

    moe_half = lax.dynamic_slice_in_dim(moe_in, core * half, half, 1)
    outgoing = jnp.dot(dispatch_rows, moe_half, preferred_element_type=jnp.float32).astype(
        jnp.bfloat16
    )
    arrived = exchanged(outgoing.reshape(experts_all, capacity, half), EP)
    own_in = arrived.reshape(slot_count, half)
    other_in = from_partner(own_in)
    own_at, other_at = core * half, (1 - core) * half

    def both_halves(weight):
        own = lax.dynamic_slice_in_dim(weight, own_at, half, 0)
        other = lax.dynamic_slice_in_dim(weight, other_at, half, 0)
        return jnp.dot(own_in, own, preferred_element_type=jnp.float32) + jnp.dot(
            other_in, other, preferred_element_type=jnp.float32
        )

    hidden = (jax.nn.silu(both_halves(expert_gate[0])) * both_halves(expert_up[0])).astype(
        jnp.bfloat16
    )

    def down_half(rows, weight, at):
        piece = lax.dynamic_slice_in_dim(weight, at, half, 1)
        return jnp.dot(rows, piece, preferred_element_type=jnp.float32).astype(jnp.bfloat16)

    def summed_half(rows, weight):
        sent = from_partner(down_half(rows, weight, other_at))
        kept = down_half(rows, weight, own_at)
        return (kept.astype(jnp.float32) + sent.astype(jnp.float32)).astype(jnp.bfloat16)

    expert_sum = summed_half(hidden, expert_down[0])
    returned = exchanged(expert_sum.reshape(experts_all, capacity, half), EP)
    back_rows = returned.reshape(slot_count, half).astype(jnp.float32)
    routed = jnp.dot(combine, back_rows)
    shared_hidden = (
        jax.nn.silu(jnp.dot(moe_in, shared_gate, preferred_element_type=jnp.float32))
        * jnp.dot(moe_in, shared_up, preferred_element_type=jnp.float32)
    ).astype(jnp.bfloat16)
    shared_out = summed_half(shared_hidden, shared_down)
    mixture = shared_out.astype(jnp.float32) + routed
    other_mixture = from_partner(mixture)
    whole = jnp.where(
        core == 0,
        jnp.concatenate([mixture, other_mixture], axis=1),
        jnp.concatenate([other_mixture, mixture], axis=1),
    )
    result = (middle + scaled_rows(whole, out_gain)).astype(jnp.bfloat16)
    return (result, new_state)


def solution(mesh):
    finer = Mesh(mesh.devices.reshape(-1, 4, 4, mesh.shape["tp"]), ("ep_0", "ep_1", "ep_2", "tp"))
    in_specs = (
        P(EP, None),
        P(EP),
        P(EP, "tp", None, None),
        P(),
        P(),
        P(),
        P(),
        P(EP, "tp"),
        P(EP, "tp"),
        P(EP, "tp"),
        P(EP, "tp"),
        P("tp", EP),
        P(EP, None),
        P(EP, None),
        P(EP, None, "tp"),
        P(EP, None, "tp"),
        P(EP, "tp", None),
        P(None, "tp"),
        P(None, "tp"),
        P("tp", None),
    )
    out_specs = (P(EP, None), P(EP, "tp", None, None))
    return jax.shard_map(
        on_device, mesh=finer, in_specs=in_specs, out_specs=out_specs, check_vma=False
    )
```

time: 291 us -> 177 us (0.61)
  waiting for transfers between devices: 170 us -> 49.4 us
  starting transfers between devices: 21 us -> 66.3 us
  blocking collectives: 44.9 us -> 25.9 us
  between operations: 15 us -> 1.18 us
  matrix products: 21.4 us -> 14 us
    all_gather x2 -> x0, waiting for transfers between devices: 132 us -> none  [the longest x1 103 us: sent_together(): out = lax.all_gather(both, axis, axis=dim, tiled=True)]
    ppermute x0 -> x11, starting transfers between devices: none -> 26.4 us  [the longest x7 20.2 us: gathered_ahead(): lax.ppermute(value, axis, [((i + j) % size, i) for i in range(size)])]
    all_gather x2 -> x0, blocking collectives: 21 us -> none  [gathered_by_axis(): value = lax.all_gather(value, axis, axis=dim, tiled=True)]
    all_to_all x3 -> x7, starting transfers between devices: 20.9 us -> 39.8 us  [exchanged(): return lax.all_to_all(blocks, axes, split_axis=0, concat_axis=0, tiled=True)]
    ppermute x0 -> x11, waiting for transfers between devices: none -> 12.9 us  [the longest x7 11 us: gathered_ahead(): lax.ppermute(value, axis, [((i + j) % size, i) for i in range(size)])]
    dot_general x8 -> x12, matrix products: 16.8 us -> 9.47 us  [the longest x2 2.7 us: both_halves(): jnp.dot(other_in, other, preferred_element_type=jnp.float32)]
    all_to_all x3 -> x1, blocking collectives: 19.5 us -> 25.9 us  [exchanged(): return lax.all_to_all(blocks, axes, split_axis=0, concat_axis=0, tiled=True)]
    unnamed x1 -> x0, blocking collectives: 4.36 us -> none
  transfers between devices with their start and end apart: 5 -> 18, of which waited for: 4 -> 10; matrix products, arithmetic and copies ran while one was open for 8% -> 11% of each run, Pallas kernels for 0% -> 0%
where the time goes in v1:
time: 177 us; the launch traced here: 176 us
  starting transfers between devices  66.3 us (37%)
  waiting for transfers between devices  49.4 us (28%)
  blocking collectives  25.9 us (15%)
  matrix products  14 us (8%)
  other arithmetic  12 us (7%)
  local copies, waits for them, and re-layouts  6.86 us (4%)
    all_to_all x7, starting transfers between devices, exchanged(): return lax.all_to_all(blocks, axes, split_axis=0, concat_axis=0, tiled=True)  39.8 us
    all_to_all x7, waiting for transfers between devices, exchanged(): return lax.all_to_all(blocks, axes, split_axis=0, concat_axis=0, tiled=True)  36.5 us
    all_to_all x1, blocking collectives, exchanged(): return lax.all_to_all(blocks, axes, split_axis=0, concat_axis=0, tiled=True)  25.9 us
    ppermute x7, starting transfers between devices, gathered_ahead(): lax.ppermute(value, axis, [((i + j) % size, i) for i in range(size)])  20.2 us
    ppermute x7, waiting for transfers between devices, gathered_ahead(): lax.ppermute(value, axis, [((i + j) % size, i) for i in range(size)])  11 us
    ppermute x4, starting transfers between devices, from_partner(): return lax.ppermute(value, 'tp', [(0, 1), (1, 0)])  6.25 us
    add x1, other arithmetic, retain(): decays[None, :, None, None] * prior_state  4.26 us
  transfers between devices with their start and end apart: 18, of which 10 were waited for; matrix products, arithmetic and copies ran while one was open for 11% of the time, Pallas kernels for 0%

profile of v1, /device:TPU:1, one launch (start us, length us, event | category | flops | bytes accessed | tf_op | source)
XLA Modules:
  0.0 175.6 jit_solution(10175175473700542124)
XLA Ops:
  0.7 1.5 pad_maximum_fusion.1
  2.2 4.8 %all-to-all-start.1 = ((bf16[4,16,512]{2,1,0:T(8,128)(2,1)}), bf16[4,16,512]{2,1,0:T(8,128)(2,1)S(1)}, u32[]{:S(2)}, u32[]{:S(2)}) async-start(bf16[4,16,512]{2,1,0:T(8,128)(2,1)} %pad_maximum_fusion.1), calls=%async_computation.1 | async-start | bytes 131072 | tf_op jit(solution)/shard_map/all_to_all | solution.py:18
  7.0 1.0 fusion.26
  8.0 0.8 copy.42
  8.9 0.9 fusion.28
  10.0 0.2 reshape.223
  10.4 1.1 all-to-all-done.1
  11.5 0.7 broadcast_in_dim.21
  12.2 5.9 %all-to-all-start = ((bf16[16,16,512]{2,1,0:T(8,128)(2,1)}), bf16[16,16,512]{2,1,0:T(8,128)(2,1)S(1)}, u32[]{:S(2)}, u32[]{:S(2)}) async-start(bf16[16,16,512]{2,1,0:T(8,128)(2,1)} %bitcast.1), calls=%async_computation | async-start | bytes 524288 | tf_op jit(solution)/shard_map/all_to_all | solution.py:18
  18.1 0.7 pad_maximum_fusion
  18.8 3.0 %collective-permute-start.5 = (bf16[80,512]{1,0:T(8,128)(2,1)S(1)}, bf16[80,512]{1,0:T(8,128)(2,1)S(1)}, u32[]{:S(2)}, u32[]{:S(2)}) collective-permute-start(bf16[80,512]{1,0:T(8,128)(2,1)S(1)} %pad_maximum_fusion), channel_id=1, source_target_pairs={{192,0},{224,32},{0,64},{32,96},{64,128},{96,160},{128,192},{160,2... | collective-permute-start | bytes 245768 | tf_op jit(solution)/shard_map/ppermute | solution.py:32
  21.8 4.7 %collective-permute-start.4 = (bf16[80,512]{1,0:T(8,128)(2,1)S(1)}, bf16[80,512]{1,0:T(8,128)(2,1)S(1)}, u32[]{:S(2)}, u32[]{:S(2)}) collective-permute-start(bf16[80,512]{1,0:T(8,128)(2,1)S(1)} %pad_maximum_fusion), channel_id=1, source_target_pairs={{160,0},{192,32},{224,64},{0,96},{32,128},{64,160},{96,192},{128,2... | collective-permute-start | bytes 245768 | tf_op jit(solution)/shard_map/ppermute | solution.py:32
  26.5 1.0 collective-permute-start.3
  27.4 3.9 %collective-permute-start.2 = (bf16[80,512]{1,0:T(8,128)(2,1)S(1)}, bf16[80,512]{1,0:T(8,128)(2,1)S(1)}, u32[]{:S(2)}, u32[]{:S(2)}) collective-permute-start(bf16[80,512]{1,0:T(8,128)(2,1)S(1)} %pad_maximum_fusion), channel_id=1, source_target_pairs={{96,0},{128,32},{160,64},{192,96},{224,128},{0,160},{32,192},{64,2... | collective-permute-start | bytes 245768 | tf_op jit(solution)/shard_map/ppermute | solution.py:32
  31.4 0.7 collective-permute-start
  32.1 0.7 bitcast_dynamic-update-slice_fusion.7
  32.8 6.0 %collective-permute-done = bf16[80,512]{1,0:T(8,128)(2,1)S(1)} collective-permute-done((bf16[80,512]{1,0:T(8,128)(2,1)S(1)}, bf16[80,512]{1,0:T(8,128)(2,1)S(1)}, u32[]{:S(2)}, u32[]{:S(2)}) %collective-permute-start) | collective-permute-done | bytes 81952 | tf_op jit(solution)/shard_map/ppermute | solution.py:32
  38.9 1.7 collective-permute-start.1
  40.6 3.6 %collective-permute-done.1 = bf16[80,512]{1,0:T(8,128)(2,1)S(1)} collective-permute-done((bf16[80,512]{1,0:T(8,128)(2,1)S(1)}, bf16[80,512]{1,0:T(8,128)(2,1)S(1)}, u32[]{:S(2)}, u32[]{:S(2)}) %collective-permute-start.1) | collective-permute-done | bytes 81952 | tf_op jit(solution)/shard_map/ppermute | solution.py:32
  44.2 5.2 %collective-permute-start.6 = (bf16[80,512]{1,0:T(8,128)(2,1)S(1)}, bf16[80,512]{1,0:T(8,128)(2,1)S(1)}, u32[]{:S(2)}, u32[]{:S(2)}) collective-permute-start(bf16[80,512]{1,0:T(8,128)(2,1)S(1)} %pad_maximum_fusion), channel_id=1, source_target_pairs={{224,0},{0,32},{32,64},{64,96},{96,128},{128,160},{160,192},{192,2... | collective-permute-start | bytes 245768 | tf_op jit(solution)/shard_map/ppermute | solution.py:32
  49.5 1.4 collective-permute-done.6
  50.9 1.0 convolution_convert_fusion.3
  51.9 6.5 %all-to-all-start.2 = ((bf16[16,16,512]{2,1,0:T(8,128)(2,1)}), bf16[16,16,512]{2,1,0:T(8,128)(2,1)S(1)}, u32[]{:S(2)}, u32[]{:S(2)}) async-start(bf16[16,16,512]{2,1,0:T(8,128)(2,1)} %bitcast.18), calls=%async_computation.2 | async-start | bytes 524288 | tf_op jit(solution)/shard_map/all_to_all | solution.py:18
  58.8 7.2 %all-to-all-done.2 = bf16[16,16,512]{2,1,0:T(8,128)(2,1)S(1)} async-done(((bf16[16,16,512]{2,1,0:T(8,128)(2,1)}), bf16[16,16,512]{2,1,0:T(8,128)(2,1)S(1)}, u32[]{:S(2)}, u32[]{:S(2)}) %all-to-all-start.2) | async-done | bytes 262176 | tf_op jit(solution)/shard_map/all_to_all | solution.py:18
  65.9 0.8 broadcast_in_dim.23
  66.8 3.5 %all-to-all-start.4 = ((bf16[4,128,512]{2,1,0:T(8,128)(2,1)}), bf16[4,128,512]{2,1,0:T(8,128)(2,1)S(1)}, u32[]{:S(2)}, u32[]{:S(2)}) async-start(bf16[4,128,512]{2,1,0:T(8,128)(2,1)} %broadcast_in_dim.23), calls=%async_computation.4 | async-start | bytes 1048576 | tf_op jit(solution)/shard_map/all_to_all | solution.py:18
  70.8 2.9 %fusion.58 = f32[16,8,1,64]{3,2,1,0:T(1,128)S(1)} fusion(f32[16,8,64,1]{2,3,1,0:T(1,128)S(1)} %bitcast.97, f32[16,8,64,64]{3,2,1,0:T(8,128)} %param.22), kind=kOutput, calls=%fused_computation.120 | convolution fusion | flops 1048576 | bytes 2162688 | tf_op jit(solution)/shard_map/shd,shde->she/dot_general | solution.py:77
  73.7 0.2 multiply_reduce_fusion.1
  74.1 3.1 %all-to-all-done.4 = bf16[4,128,512]{2,1,0:T(8,128)(2,1)S(1)} async-done(((bf16[4,128,512]{2,1,0:T(8,128)(2,1)}), bf16[4,128,512]{2,1,0:T(8,128)(2,1)S(1)}, u32[]{:S(2)}, u32[]{:S(2)}) %all-to-all-start.4) | async-done | bytes 524320 | tf_op jit(solution)/shard_map/all_to_all | solution.py:18
  77.1 0.6 broadcast_in_dim.22
  77.8 3.3 %all-to-all-start.3 = ((bf16[4,16,512]{2,1,0:T(8,128)(2,1)}), bf16[4,16,512]{2,1,0:T(8,128)(2,1)S(1)}, u32[]{:S(2)}, u32[]{:S(2)}) async-start(bf16[4,16,512]{2,1,0:T(8,128)(2,1)} %broadcast_in_dim.22), calls=%async_computation.3 | async-start | bytes 131072 | tf_op jit(solution)/shard_map/all_to_all | solution.py:18
  81.1 0.2 select_reduce_fusion.1
  81.5 4.0 %all-to-all-done.3 = bf16[4,16,512]{2,1,0:T(8,128)(2,1)S(1)} async-done(((bf16[4,16,512]{2,1,0:T(8,128)(2,1)}), bf16[4,16,512]{2,1,0:T(8,128)(2,1)S(1)}, u32[]{:S(2)}, u32[]{:S(2)}) %all-to-all-start.3) | async-done | bytes 65568 | tf_op jit(solution)/shard_map/all_to_all | solution.py:18
  85.5 0.3 convolution_convert_fusion.4
  85.8 0.7 broadcast_in_dim.25
  86.5 9.7 %all-to-all-start.5 = ((bf16[8,16,512]{2,1,0:T(8,128)(2,1)}), bf16[8,16,512]{2,1,0:T(8,128)(2,1)S(1)}, u32[]{:S(2)}, u32[]{:S(2)}) async-start(bf16[8,16,512]{2,1,0:T(8,128)(2,1)} %bitcast.32), calls=%async_computation.5 | async-start | bytes 262144 | tf_op jit(solution)/shard_map/all_to_all | solution.py:18
  96.3 5.2 %all-to-all-done.5 = bf16[8,16,512]{2,1,0:T(8,128)(2,1)S(1)} async-done(((bf16[8,16,512]{2,1,0:T(8,128)(2,1)}), bf16[8,16,512]{2,1,0:T(8,128)(2,1)S(1)}, u32[]{:S(2)}, u32[]{:S(2)}) %all-to-all-start.5) | async-done | bytes 131104 | tf_op jit(solution)/shard_map/all_to_all | solution.py:18
  101.5 0.2 reshape.236
  101.8 0.2 reshape.237
  102.6 0.3 convolution_convert_fusion.2
  103.0 0.2 reshape.238
  103.2 25.9 %all_to_all.40 = bf16[128,2,1024]{2,1,0:T(2,128)(2,1)S(1)} all-to-all(bf16[128,2,1024]{2,1,0:T(2,128)(2,1)S(1)} %reshape.238), channel_id=1, replica_groups=mesh['ep_0'=8,'ep_1'=4,'ep_2'=4,'tp'=2] {'ep_0','ep_1','ep_2'}, dimensions={0} | all-to-all | bytes 1048576 | tf_op jit(solution)/shard_map/all_to_all | solution.py:18
  129.1 0.2 reshape.239
  129.3 3.6 %collective-permute-start.8 = (bf16[256,1024]{1,0:T(8,128)(2,1)S(1)}, bf16[256,1024]{1,0:T(8,128)(2,1)S(1)}, u32[]{:S(2)}, u32[]{:S(2)}) collective-permute-start(bf16[256,1024]{1,0:T(8,128)(2,1)S(1)} %reshape.239), channel_id=1, source_target_pairs={{0,1},{1,0},{2,3},{3,2},{4,5},{5,4},{6,7},{7,6},{8,9},{9,8},{10,11... | collective-permute-start | bytes 1572872 | tf_op jit(solution)/shard_map/ppermute | solution.py:26
  132.9 1.3 fusion.11
  134.3 1.3 fusion.14
  135.6 1.3 convolution_add_fusion.1
  137.0 1.4 multiply_convert_fusion
  138.4 0.3 convolution_convert_fusion
  138.8 1.9 %collective-permute-done.9 = bf16[256,1024]{1,0:T(8,128)(2,1)S(1)} collective-permute-done((bf16[256,1024]{1,0:T(8,128)(2,1)S(1)}, bf16[256,1024]{1,0:T(8,128)(2,1)S(1)}, u32[]{:S(2)}, u32[]{:S(2)}) %collective-permute-start.9) | collective-permute-done | bytes 524320 | tf_op jit(solution)/shard_map/ppermute | solution.py:26
  140.7 0.3 add_convert_fusion
  141.0 1.0 reshape.240
  142.0 6.2 %all-to-all-start.7 = ((bf16[128,2,1024]{2,1,0:T(2,128)(2,1)}), bf16[128,2,1024]{2,1,0:T(2,128)(2,1)S(1)}, u32[]{:S(2)}, u32[]{:S(2)}) async-start(bf16[128,2,1024]{2,1,0:T(2,128)(2,1)} %reshape.240), calls=%async_computation.7 | async-start | bytes 1048576 | tf_op jit(solution)/shard_map/all_to_all | solution.py:18
  148.3 1.5 fusion.59
  149.8 1.5 fusion.5
  151.2 0.2 convolution_convert_fusion.5
  151.4 0.2 collective-permute-start.7
  151.6 16.0 %all-to-all-done.7 = bf16[128,2,1024]{2,1,0:T(2,128)(2,1)S(1)} async-done(((bf16[128,2,1024]{2,1,0:T(2,128)(2,1)}), bf16[128,2,1024]{2,1,0:T(2,128)(2,1)S(1)}, u32[]{:S(2)}, u32[]{:S(2)}) %all-to-all-start.7) | async-done | bytes 524320 | tf_op jit(solution)/shard_map/all_to_all | solution.py:18
  167.5 0.2 reshape.241
  167.7 0.2 fusion.60
  167.9 0.2 convert_add_fusion.2
  168.1 2.4 %collective-permute-start.10 = (f32[16,1024]{1,0:T(8,128)S(1)}, f32[16,1024]{1,0:T(8,128)S(1)}, u32[]{:S(2)}, u32[]{:S(2)}) collective-permute-start(f32[16,1024]{1,0:T(8,128)S(1)} %convert_add_fusion.2), channel_id=1, source_target_pairs={{0,1},{1,0},{2,3},{3,2},{4,5},{5,4},{6,7},{7,6},{8,9},{9,8},{10,11... | collective-permute-start | bytes 196616 | tf_op jit(solution)/shard_map/ppermute | solution.py:26
  170.5 4.3 %multiply_add_fusion = f32[16,8,64,64]{3,2,1,0:T(8,128)} fusion(f32[16,8,64,64]{3,2,1,0:T(8,128)} %param.22, f32[16,8,64]{2,1,0:T(8,128)S(1)} %reshape.244, f32[16,8,64]{2,1,0:T(8,128)S(1)} %get-tuple-element.16, f32[8]{0:T(128)S(1)} %dynamic_slice.48), kind=kLoop, calls=%fused_computation.1 | loop fusion | flops 1572864 | bytes 4259872 | tf_op jit(solution)/shard_map/add | solution.py:81
  174.9 0.7 fusion.33
  (76 shorter events, 3.1 us)
Async XLA Ops:
  0.6 137.7 %copy-start = (bf16[1,256,2048]{2,1,0:T(8,128)(2,1)S(1)}, bf16[1,256,2048]{2,1,0:T(8,128)(2,1)}, u32[]{:S(2)}) copy-start(bf16[1,256,2048]{2,1,0:T(8,128)(2,1)} %param.36) | copy-start | bytes 3145732
  0.6 57.7 %copy-start.8 = (s32[16]{0:T(128)S(1)}, s32[16]{0:T(128)}, u32[]{:S(2)}) copy-start(s32[16]{0:T(128)} %param.21) | copy-start | bytes 196
  2.2 9.3 %all-to-all-start.1 = ((bf16[4,16,512]{2,1,0:T(8,128)(2,1)}), bf16[4,16,512]{2,1,0:T(8,128)(2,1)S(1)}, u32[]{:S(2)}, u32[]{:S(2)}) async-start(bf16[4,16,512]{2,1,0:T(8,128)(2,1)} %pad_maximum_fusion.1), calls=%async_computation.1 | async-start | bytes 131072 | tf_op jit(solution)/shard_map/all_to_all | solution.py:18
  12.2 38.7 %all-to-all-start = ((bf16[16,16,512]{2,1,0:T(8,128)(2,1)}), bf16[16,16,512]{2,1,0:T(8,128)(2,1)S(1)}, u32[]{:S(2)}, u32[]{:S(2)}) async-start(bf16[16,16,512]{2,1,0:T(8,128)(2,1)} %bitcast.1), calls=%async_computation | async-start | bytes 524288 | tf_op jit(solution)/shard_map/all_to_all | solution.py:18
  18.8 30.6 %collective-permute-start.5 = (bf16[80,512]{1,0:T(8,128)(2,1)S(1)}, bf16[80,512]{1,0:T(8,128)(2,1)S(1)}, u32[]{:S(2)}, u32[]{:S(2)}) collective-permute-start(bf16[80,512]{1,0:T(8,128)(2,1)S(1)} %pad_maximum_fusion), channel_id=1, source_target_pairs={{192,0},{224,32},{0,64},{32,96},{64,128},{96,160},{128,192},{160,2... | collective-permute-start | bytes 245768 | tf_op jit(solution)/shard_map/ppermute | solution.py:32
  21.8 27.6 %collective-permute-start.4 = (bf16[80,512]{1,0:T(8,128)(2,1)S(1)}, bf16[80,512]{1,0:T(8,128)(2,1)S(1)}, u32[]{:S(2)}, u32[]{:S(2)}) collective-permute-start(bf16[80,512]{1,0:T(8,128)(2,1)S(1)} %pad_maximum_fusion), channel_id=1, source_target_pairs={{160,0},{192,32},{224,64},{0,96},{32,128},{64,160},{96,192},{128,2... | collective-permute-start | bytes 245768 | tf_op jit(solution)/shard_map/ppermute | solution.py:32
  26.5 22.9 %collective-permute-start.3 = (bf16[80,512]{1,0:T(8,128)(2,1)S(1)}, bf16[80,512]{1,0:T(8,128)(2,1)S(1)}, u32[]{:S(2)}, u32[]{:S(2)}) collective-permute-start(bf16[80,512]{1,0:T(8,128)(2,1)S(1)} %pad_maximum_fusion), channel_id=1, source_target_pairs={{128,0},{160,32},{192,64},{224,96},{0,128},{32,160},{64,192},{96,2... | collective-permute-start | bytes 245768 | tf_op jit(solution)/shard_map/ppermute | solution.py:32
  27.4 21.9 %collective-permute-start.2 = (bf16[80,512]{1,0:T(8,128)(2,1)S(1)}, bf16[80,512]{1,0:T(8,128)(2,1)S(1)}, u32[]{:S(2)}, u32[]{:S(2)}) collective-permute-start(bf16[80,512]{1,0:T(8,128)(2,1)S(1)} %pad_maximum_fusion), channel_id=1, source_target_pairs={{96,0},{128,32},{160,64},{192,96},{224,128},{0,160},{32,192},{64,2... | collective-permute-start | bytes 245768 | tf_op jit(solution)/shard_map/ppermute | solution.py:32
  31.4 7.5 %collective-permute-start = (bf16[80,512]{1,0:T(8,128)(2,1)S(1)}, bf16[80,512]{1,0:T(8,128)(2,1)S(1)}, u32[]{:S(2)}, u32[]{:S(2)}) collective-permute-start(bf16[80,512]{1,0:T(8,128)(2,1)S(1)} %pad_maximum_fusion), channel_id=1, source_target_pairs={{32,0},{64,32},{96,64},{128,96},{160,128},{192,160},{224,192},{0,2... | collective-permute-start | bytes 245768 | tf_op jit(solution)/shard_map/ppermute | solution.py:32
  38.9 5.3 %collective-permute-start.1 = (bf16[80,512]{1,0:T(8,128)(2,1)S(1)}, bf16[80,512]{1,0:T(8,128)(2,1)S(1)}, u32[]{:S(2)}, u32[]{:S(2)}) collective-permute-start(bf16[80,512]{1,0:T(8,128)(2,1)S(1)} %pad_maximum_fusion), channel_id=1, source_target_pairs={{64,0},{96,32},{128,64},{160,96},{192,128},{224,160},{0,192},{32,2... | collective-permute-start | bytes 245768 | tf_op jit(solution)/shard_map/ppermute | solution.py:32
  44.2 6.6 %collective-permute-start.6 = (bf16[80,512]{1,0:T(8,128)(2,1)S(1)}, bf16[80,512]{1,0:T(8,128)(2,1)S(1)}, u32[]{:S(2)}, u32[]{:S(2)}) collective-permute-start(bf16[80,512]{1,0:T(8,128)(2,1)S(1)} %pad_maximum_fusion), channel_id=1, source_target_pairs={{224,0},{0,32},{32,64},{64,96},{96,128},{128,160},{160,192},{192,2... | collective-permute-start | bytes 245768 | tf_op jit(solution)/shard_map/ppermute | solution.py:32
  51.9 14.0 %all-to-all-start.2 = ((bf16[16,16,512]{2,1,0:T(8,128)(2,1)}), bf16[16,16,512]{2,1,0:T(8,128)(2,1)S(1)}, u32[]{:S(2)}, u32[]{:S(2)}) async-start(bf16[16,16,512]{2,1,0:T(8,128)(2,1)} %bitcast.18), calls=%async_computation.2 | async-start | bytes 524288 | tf_op jit(solution)/shard_map/all_to_all | solution.py:18
  66.8 10.4 %all-to-all-start.4 = ((bf16[4,128,512]{2,1,0:T(8,128)(2,1)}), bf16[4,128,512]{2,1,0:T(8,128)(2,1)S(1)}, u32[]{:S(2)}, u32[]{:S(2)}) async-start(bf16[4,128,512]{2,1,0:T(8,128)(2,1)} %broadcast_in_dim.23), calls=%async_computation.4 | async-start | bytes 1048576 | tf_op jit(solution)/shard_map/all_to_all | solution.py:18
  70.5 25.6 %copy-start.3 = (s32[16,6]{0,1:T(8,128)S(1)}, s32[16,6]{0,1:T(8,128)}, u32[]{:S(2)}) copy-start(s32[16,6]{0,1:T(8,128)} %param.32) | copy-start | bytes 1156
  70.8 31.5 %copy-start.2 = (bf16[16,2048]{1,0:T(8,128)(2,1)S(1)}, bf16[16,2048]{1,0:T(8,128)(2,1)}, u32[]{:S(2)}) copy-start(bf16[16,2048]{1,0:T(8,128)(2,1)} %param.20) | copy-start | bytes 196612
  70.8 31.5 %copy-start.4 = (f32[2048]{0:T(1024)S(1)}, f32[2048]{0:T(1024)}, u32[]{:S(2)}) copy-start(f32[2048]{0:T(1024)} %param.24) | copy-start | bytes 24580
  70.8 31.8 %copy-start.5 = (f32[2048]{0:T(1024)S(1)}, f32[2048]{0:T(1024)}, u32[]{:S(2)}) copy-start(f32[2048]{0:T(1024)} %param.25) | copy-start | bytes 24580
  77.8 7.7 %all-to-all-start.3 = ((bf16[4,16,512]{2,1,0:T(8,128)(2,1)}), bf16[4,16,512]{2,1,0:T(8,128)(2,1)S(1)}, u32[]{:S(2)}, u32[]{:S(2)}) async-start(bf16[4,16,512]{2,1,0:T(8,128)(2,1)} %broadcast_in_dim.22), calls=%async_computation.3 | async-start | bytes 131072 | tf_op jit(solution)/shard_map/all_to_all | solution.py:18
  86.5 15.0 %all-to-all-start.5 = ((bf16[8,16,512]{2,1,0:T(8,128)(2,1)}), bf16[8,16,512]{2,1,0:T(8,128)(2,1)S(1)}, u32[]{:S(2)}, u32[]{:S(2)}) async-start(bf16[8,16,512]{2,1,0:T(8,128)(2,1)} %bitcast.32), calls=%async_computation.5 | async-start | bytes 262144 | tf_op jit(solution)/shard_map/all_to_all | solution.py:18
  129.3 6.3 %collective-permute-start.8 = (bf16[256,1024]{1,0:T(8,128)(2,1)S(1)}, bf16[256,1024]{1,0:T(8,128)(2,1)S(1)}, u32[]{:S(2)}, u32[]{:S(2)}) collective-permute-start(bf16[256,1024]{1,0:T(8,128)(2,1)S(1)} %reshape.239), channel_id=1, source_target_pairs={{0,1},{1,0},{2,3},{3,2},{4,5},{5,4},{6,7},{7,6},{8,9},{9,8},{10,11... | collective-permute-start | bytes 1572872 | tf_op jit(solution)/shard_map/ppermute | solution.py:26
  135.6 12.6 %copy-start.7 = (f32[16,6]{0,1:T(8,128)S(1)}, f32[16,6]{0,1:T(8,128)}, u32[]{:S(2)}) copy-start(f32[16,6]{0,1:T(8,128)} %param.33) | copy-start | bytes 1156
  138.4 12.9 %copy-start.1 = (bf16[256,2048]{1,0:T(8,128)(2,1)S(1)}, bf16[256,2048]{1,0:T(8,128)(2,1)}, u32[]{:S(2)}) copy-start(bf16[256,2048]{1,0:T(8,128)(2,1)} %param.39) | copy-start | bytes 3145732
  138.7 2.0 %collective-permute-start.9 = (bf16[256,1024]{1,0:T(8,128)(2,1)S(1)}, bf16[256,1024]{1,0:T(8,128)(2,1)S(1)}, u32[]{:S(2)}, u32[]{:S(2)}) collective-permute-start(bf16[256,1024]{1,0:T(8,128)(2,1)S(1)} %convolution_convert_fusion), channel_id=1, source_target_pairs={{0,1},{1,0},{2,3},{3,2},{4,5},{5,4},{6,7},{7,6},{8,9},{9,8},{10,11... | collective-permute-start | bytes 1572872 | tf_op jit(solution)/shard_map/ppermute | solution.py:26
  142.0 25.6 %all-to-all-start.7 = ((bf16[128,2,1024]{2,1,0:T(2,128)(2,1)}), bf16[128,2,1024]{2,1,0:T(2,128)(2,1)S(1)}, u32[]{:S(2)}, u32[]{:S(2)}) async-start(bf16[128,2,1024]{2,1,0:T(2,128)(2,1)} %reshape.240), calls=%async_computation.7 | async-start | bytes 1048576 | tf_op jit(solution)/shard_map/all_to_all | solution.py:18
  151.4 16.5 %collective-permute-start.7 = (bf16[16,1024]{1,0:T(8,128)(2,1)S(1)}, bf16[16,1024]{1,0:T(8,128)(2,1)S(1)}, u32[]{:S(2)}, u32[]{:S(2)}) collective-permute-start(bf16[16,1024]{1,0:T(8,128)(2,1)S(1)} %convolution_convert_fusion.5), channel_id=1, source_target_pairs={{0,1},{1,0},{2,3},{3,2},{4,5},{5,4},{6,7},{7,6},{8,9},{9,8},{10,11... | collective-permute-start | bytes 98312 | tf_op jit(solution)/shard_map/ppermute | solution.py:26
  168.1 6.8 %copy-start.6 = (f32[2048]{0:T(1024)S(1)}, f32[2048]{0:T(1024)}, u32[]{:S(2)}) copy-start(f32[2048]{0:T(1024)} %param.26) | copy-start | bytes 24580
  168.1 6.6 %collective-permute-start.10 = (f32[16,1024]{1,0:T(8,128)S(1)}, f32[16,1024]{1,0:T(8,128)S(1)}, u32[]{:S(2)}, u32[]{:S(2)}) collective-permute-start(f32[16,1024]{1,0:T(8,128)S(1)} %convert_add_fusion.2), channel_id=1, source_target_pairs={{0,1},{1,0},{2,3},{3,2},{4,5},{5,4},{6,7},{7,6},{8,9},{9,8},{10,11... | collective-permute-start | bytes 196616 | tf_op jit(solution)/shard_map/ppermute | solution.py:26

commit v2 on v1

--- a/solution.py
+++ b/solution.py
@@ -26,18 +26,29 @@
     return lax.ppermute(value, "tp", [(0, 1), (1, 0)])
 
 
-def gathered_ahead(value, axis):
+def from_ahead(value, axis, step):
     size = lax.axis_size(axis)
-    others = [
-        lax.ppermute(value, axis, [((i + j) % size, i) for i in range(size)])
-        for j in range(1, size)
-    ]
-    return jnp.stack([value, *others])
-
-
-def rolled_lanes(rows, start):
-    doubled = jnp.concatenate([rows, rows], axis=1)
-    return lax.dynamic_slice_in_dim(doubled, start, rows.shape[1], 1)
+    return lax.ppermute(value, axis, [((i + step) % size, i) for i in range(size)])
+
+
+def in_place_order(blocks, axis, dim):
+    size = blocks.shape[dim]
+    doubled = jnp.concatenate([blocks, blocks], axis=dim)
+    start = (size - lax.axis_index(axis)) % size
+    return lax.dynamic_slice_in_dim(doubled, start, size, dim)
+
+
+def plane_tokens(by_y):
+    size_y, size_x = by_y.shape[0], lax.axis_size(X)
+    mine = lax.axis_index(Y)
+    column = [lax.dynamic_index_in_dim(by_y, mine, 0, keepdims=False)]
+    for step in range(1, size_y):
+        behind = (mine - step) % size_y
+        block = lax.dynamic_index_in_dim(by_y, behind, 0, keepdims=False)
+        column.append(from_ahead(block, Y, step))
+    column = in_place_order(jnp.stack(column), Y, 0)
+    plane = jnp.stack([column] + [from_ahead(column, X, step) for step in range(1, size_x)])
+    return in_place_order(plane, X, 0).swapaxes(0, 1)
 
 
 def rounded(values):
@@ -115,26 +126,20 @@
     depth, rows_y, rows_x = (lax.axis_size(axis) for axis in EP)
     experts_all = depth * rows_y * rows_x
     plane = rows_y * rows_x
-    mine_z = lax.axis_index(Z)
     core = lax.axis_index("tp")
-    slab = width // depth
     half = width // 2
 
     kinds = jnp.stack([query_weight, key_weight, value_weight, gate_weight])
-    my_kind = exchanged(kinds, X)
-    wout_rows = out_weight.T
-    shard = jnp.concatenate([my_kind.reshape(-1, cols), wout_rows], axis=0)
-    ahead = gathered_ahead(shard, Z)
-    kind_rows = my_kind.shape[0] * my_kind.shape[1]
-    kind_weight = ahead[:, :kind_rows].reshape(-1, cols)
-    wout_z = ahead[:, kind_rows:]
+    wout_rows = copies(out_weight.T, rows_x)
+    sent = copies(jnp.concatenate([kinds, wout_rows], axis=1), depth)
+    held = exchanged(sent.reshape(depth * rows_x, -1, cols), (Z, X))
+    kind_rows = query_weight.shape[0]
+    kind_weight = held[:, :kind_rows].reshape(-1, cols)
+    wout_zx = held[:, kind_rows:].reshape(-1, cols)
 
     normed = scaled_rows(tokens, mix_gain).astype(jnp.bfloat16)
-    turned = rolled_lanes(normed, mine_z * slab)
-    by_y = turned.reshape(seq_here, depth, rows_y, -1).transpose(2, 0, 1, 3)
-    by_y = by_y.reshape(rows_y, 1, seq_here, width // rows_y)
-    outgoing_rows = jnp.broadcast_to(by_y, (rows_y, rows_x, seq_here, width // rows_y))
-    plane_rows = exchanged(outgoing_rows.reshape(plane, seq_here, -1), (Y, X))
+    by_y = normed.reshape(seq_here, depth, rows_y, -1).transpose(2, 0, 1, 3)
+    plane_rows = plane_tokens(by_y.reshape(rows_y, seq_here, width // rows_y))
     projected = jnp.dot(
         plane_rows.reshape(plane * seq_here, -1), kind_weight, preferred_element_type=jnp.float32
     ).astype(jnp.bfloat16)
@@ -146,8 +151,6 @@
     decays = lax.dynamic_slice_in_dim(decay_table(HEADS), core * heads_here, heads_here, 0)
     retained, new_state = retain(queries, keys_new, values, out_gate, prior_state, lengths, decays)
 
-    wout_zx = exchanged(copies(wout_z.reshape(-1, cols), rows_x), X)
-    wout_zx = wout_zx.reshape(rows_x, depth, -1, cols).transpose(1, 0, 2, 3).reshape(-1, cols)
     retained_y = exchanged(copies(retained, rows_y), Y).reshape(rows_y * seq_here, cols)
     partial_mix = lax.dot_general(
         retained_y, wout_zx, (((1,), (1,)), ((), ())), preferred_element_type=jnp.float32
@@ -158,7 +161,7 @@
     halves = halves.reshape(rows_y, 2, seq_here, depth, -1).astype(jnp.float32)
     mixed = jnp.sum(halves, axis=1).astype(jnp.bfloat16)
     mixed = mixed.transpose(1, 2, 0, 3).reshape(seq_here, width)
-    mixed_sum = rounded(rolled_lanes(mixed, (depth - mine_z) * slab))
+    mixed_sum = rounded(mixed)
     middle = rounded(tokens.astype(jnp.float32) + scaled_rows(mixed_sum, post_gain))
     moe_in = scaled_rows(middle, ffn_gain).astype(jnp.bfloat16)
 
@@ -185,39 +188,47 @@
         jnp.bfloat16
     )
     arrived = exchanged(outgoing.reshape(experts_all, capacity, half), EP)
-    own_in = arrived.reshape(slot_count, half)
-    other_in = from_partner(own_in)
     own_at, other_at = core * half, (1 - core) * half
 
-    def both_halves(weight):
-        own = lax.dynamic_slice_in_dim(weight, own_at, half, 0)
-        other = lax.dynamic_slice_in_dim(weight, other_at, half, 0)
-        return jnp.dot(own_in, own, preferred_element_type=jnp.float32) + jnp.dot(
-            other_in, other, preferred_element_type=jnp.float32
+    def down_halves(weight):
+        return tuple(lax.dynamic_slice_in_dim(weight, at, half, 1) for at in (own_at, other_at))
+
+    def up_halves():
+        both = (expert_gate[0], expert_up[0])
+        return tuple(
+            jnp.concatenate([lax.dynamic_slice_in_dim(w, at, half, 0) for w in both], axis=1)
+            for at in (own_at, other_at)
         )
 
-    hidden = (jax.nn.silu(both_halves(expert_gate[0])) * both_halves(expert_up[0])).astype(
-        jnp.bfloat16
-    )
-
-    def down_half(rows, weight, at):
-        piece = lax.dynamic_slice_in_dim(weight, at, half, 1)
-        return jnp.dot(rows, piece, preferred_element_type=jnp.float32).astype(jnp.bfloat16)
-
-    def summed_half(rows, weight):
-        sent = from_partner(down_half(rows, weight, other_at))
-        kept = down_half(rows, weight, own_at)
-        return (kept.astype(jnp.float32) + sent.astype(jnp.float32)).astype(jnp.bfloat16)
-
-    expert_sum = summed_half(hidden, expert_down[0])
-    returned = exchanged(expert_sum.reshape(experts_all, capacity, half), EP)
-    back_rows = returned.reshape(slot_count, half).astype(jnp.float32)
-    routed = jnp.dot(combine, back_rows)
+    def summed_half(rows, halves):
+        kept, sent = (
+            jnp.dot(rows, piece, preferred_element_type=jnp.float32).astype(jnp.bfloat16)
+            for piece in halves
+        )
+        got = from_partner(sent)
+        return (kept.astype(jnp.float32) + got.astype(jnp.float32)).astype(jnp.bfloat16)
+
     shared_hidden = (
         jax.nn.silu(jnp.dot(moe_in, shared_gate, preferred_element_type=jnp.float32))
         * jnp.dot(moe_in, shared_up, preferred_element_type=jnp.float32)
     ).astype(jnp.bfloat16)
-    shared_out = summed_half(shared_hidden, shared_down)
+    shared_out = summed_half(shared_hidden, down_halves(shared_down))
+
+    beside = (shared_out, new_state, up_halves(), down_halves(expert_down[0]))
+    arrived, beside = lax.optimization_barrier((arrived, beside))
+    shared_out, new_state, up_pieces, down_pieces = beside
+
+    own_in = arrived.reshape(slot_count, half)
+    other_in = from_partner(own_in)
+    lifted = jnp.dot(own_in, up_pieces[0], preferred_element_type=jnp.float32) + jnp.dot(
+        other_in, up_pieces[1], preferred_element_type=jnp.float32
+    )
+    gate_part, up_part = jnp.split(lifted, 2, axis=1)
+    hidden = (jax.nn.silu(gate_part) * up_part).astype(jnp.bfloat16)
+    expert_sum = summed_half(hidden, down_pieces)
+    returned = exchanged(expert_sum.reshape(experts_all, capacity, half), EP)
+    back_rows = returned.reshape(slot_count, half).astype(jnp.float32)
+    routed = jnp.dot(combine, back_rows)
     mixture = shared_out.astype(jnp.float32) + routed
     other_mixture = from_partner(mixture)
     whole = jnp.where(
@@ -254,6 +265,7 @@
         P("tp", None),
     )
     out_specs = (P(EP, None), P(EP, "tp", None, None))
+
     return jax.shard_map(
         on_device, mesh=finer, in_specs=in_specs, out_specs=out_specs, check_vma=False
     )

time: 177 us -> 169 us (0.955)
  blocking collectives: 25.9 us -> 0 us
  waiting for transfers between devices: 49.4 us -> 63.9 us
  local copies, waits for them, and re-layouts: 6.86 us -> 17.8 us
  starting transfers between devices: 66.3 us -> 59.3 us
    all_to_all x1 -> x0, blocking collectives: 25.9 us -> none  [exchanged(): return lax.all_to_all(blocks, axes, split_axis=0, concat_axis=0, tiled=True)]
    all_to_all x7 -> x6, waiting for transfers between devices: 36.5 us -> 57.2 us  [exchanged(): return lax.all_to_all(blocks, axes, split_axis=0, concat_axis=0, tiled=True)]
    ppermute x7 -> x6, starting transfers between devices: 20.2 us -> 10.2 us  [from_ahead(): lax.ppermute(value, axis, [((i + step) % size, i) for i in range(size)])]
    ppermute x7 -> x6, waiting for transfers between devices: 11 us -> 3.92 us  [from_ahead(): lax.ppermute(value, axis, [((i + step) % size, i) for i in range(size)])]
    dynamic_slice x0 -> x2, local copies, waits for them, and re-layouts: none -> 4.95 us  [the longest x1 2.7 us: up_halves(): lax.dynamic_slice_in_dim(w, at, half, 0)]
    dot_general x8 -> x6, matrix products: 6.37 us -> 2.89 us  [the longest x1 1.47 us: on_device(): jnp.dot(own_in, up_pieces[0], preferred_element_type=jnp.float32)]
    all_to_all x7 -> x6, starting transfers between devices: 39.8 us -> 42 us  [exchanged(): return lax.all_to_all(blocks, axes, split_axis=0, concat_axis=0, tiled=True)]
    reshape x1, local copies, waits for them, and re-layouts: 0.2 us -> 2.04 us  [on_device(): own_in = arrived.reshape(slot_count, half)]
  transfers between devices with their start and end apart: 18 -> 16, of which waited for: 10 -> 12; matrix products, arithmetic and copies ran while one was open for 11% -> 11% of each run, Pallas kernels for 0% -> 0%
where the time goes in v2:
time: 169 us; the launch traced here: 168 us
  waiting for transfers between devices  63.9 us (38%)
  starting transfers between devices  59.3 us (35%)
  local copies, waits for them, and re-layouts  17.8 us (11%)
  other arithmetic  13.3 us (8%)
  matrix products  12.3 us (7%)
    all_to_all x6, waiting for transfers between devices, exchanged(): return lax.all_to_all(blocks, axes, split_axis=0, concat_axis=0, tiled=True)  57.2 us
    all_to_all x6, starting transfers between devices, exchanged(): return lax.all_to_all(blocks, axes, split_axis=0, concat_axis=0, tiled=True)  42 us
    ppermute x6, starting transfers between devices, from_ahead(): lax.ppermute(value, axis, [((i + step) % size, i) for i in range(size)])  10.2 us
    ppermute x4, starting transfers between devices, from_partner(): return lax.ppermute(value, 'tp', [(0, 1), (1, 0)])  7.02 us
    add x1, other arithmetic, retain(): decays[None, :, None, None] * prior_state  4.26 us
    ppermute x6, waiting for transfers between devices, from_ahead(): lax.ppermute(value, axis, [((i + step) % size, i) for i in range(size)])  3.92 us
  transfers between devices with their start and end apart: 16, of which 12 were waited for; matrix products, arithmetic and copies ran while one was open for 11% of the time, Pallas kernels for 0%

profile of v2, /device:TPU:1, one launch (start us, length us, event | category | flops | bytes accessed | tf_op | source)
XLA Modules:
  0.0 167.7 jit_solution(13170698730014659400)
XLA Ops:
  0.7 1.0 fusion.11
  1.8 0.9 fusion.13
  3.1 2.2 %collective-permute-start.2 = (bf16[16,512]{1,0:T(8,128)(2,1)S(1)}, bf16[16,512]{1,0:T(8,128)(2,1)S(1)}, u32[]{:S(2)}, u32[]{:S(2)}) collective-permute-start(bf16[16,512]{1,0:T(8,128)(2,1)S(1)} %get-tuple-element.33), channel_id=1, source_target_pairs={{24,0},{0,8},{8,16},{16,24},{25,1},{1,9},{9,17},{17,25},{26,2},{2,... | collective-permute-start | bytes 49160 | tf_op jit(solution)/shard_map/ppermute | solution.py:31
  5.3 2.6 %collective-permute-start.1 = (bf16[16,512]{1,0:T(8,128)(2,1)S(1)}, bf16[16,512]{1,0:T(8,128)(2,1)S(1)}, u32[]{:S(2)}, u32[]{:S(2)}) collective-permute-start(bf16[16,512]{1,0:T(8,128)(2,1)S(1)} %get-tuple-element.35), channel_id=1, source_target_pairs={{16,0},{24,8},{0,16},{8,24},{17,1},{25,9},{1,17},{9,25},{18,2},{26... | collective-permute-start | bytes 49160 | tf_op jit(solution)/shard_map/ppermute | solution.py:31
  7.9 1.1 collective-permute-start
  9.0 0.7 broadcast_in_dim.18
  9.7 0.8 pad_maximum_fusion.2
  10.5 1.1 broadcast_in_dim.19
  11.6 11.0 %all-to-all-start = ((bf16[32,32,512]{2,1,0:T(8,128)(2,1)}), bf16[32,32,512]{2,1,0:T(8,128)(2,1)S(1)}, u32[]{:S(2)}, u32[]{:S(2)}) async-start(bf16[32,32,512]{2,1,0:T(8,128)(2,1)} %bitcast.18), calls=%async_computation | async-start | bytes 2097152 | tf_op jit(solution)/shard_map/all_to_all | solution.py:18
  23.4 2.7 %dynamic-slice_bitcast_fusion.2 = (bf16[1024,256]{1,0:T(8,128)(2,1)S(1)}, bf16[1024,256]{1,0:T(8,128)(2,1)}, bf16[1024,256]{1,0:T(8,128)(2,1)}, bf16[1024,256]{1,0:T(8,128)(2,1)S(1)}) fusion(bf16[1,2048,256]{2,1,0:T(8,128)(2,1)} %param.35, s32[]{:T(128)S(6)} %select_n.84, s32[]{:T(128)S(6)} %select_n.83, bf16[1,2048,256]{2,1,0:T(8,128)(2,1)} %param.34), kind=kLoop, calls=%fused_computation.22 | loop fusion | bytes 4194312 | tf_op jit(solution)/shard_map/dynamic_slice | solution.py:199
  26.1 2.3 %dynamic-slice_bitcast_fusion = (bf16[256,1024]{1,0:T(8,128)(2,1)}, bf16[256,1024]{1,0:T(8,128)(2,1)}) fusion(bf16[1,256,2048]{2,1,0:T(8,128)(2,1)} %param.36, s32[]{:T(128)S(6)} %select_n.84, s32[]{:T(128)S(6)} %select_n.83), kind=kLoop, calls=%fused_computation.20 | loop fusion | bytes 2097160 | tf_op jit(solution)/shard_map/dynamic_slice | solution.py:194
  28.5 2.5 %collective-permute-start.3 = (bf16[4,16,512]{2,1,0:T(8,128)(2,1)S(1)}, bf16[4,16,512]{2,1,0:T(8,128)(2,1)S(1)}, u32[]{:S(2)}, u32[]{:S(2)}) collective-permute-start(bf16[4,16,512]{2,1,0:T(8,128)(2,1)S(1)} %get-tuple-element.17), channel_id=1, source_target_pairs={{2,0},{4,2},{6,4},{0,6},{3,1},{5,3},{7,5},{1,7},{10,8},{12,10},{14... | collective-permute-start | bytes 196616 | tf_op jit(solution)/shard_map/ppermute | solution.py:31
  31.1 1.7 %collective-permute-start.4 = (bf16[4,16,512]{2,1,0:T(8,128)(2,1)S(1)}, bf16[4,16,512]{2,1,0:T(8,128)(2,1)S(1)}, u32[]{:S(2)}, u32[]{:S(2)}) collective-permute-start(bf16[4,16,512]{2,1,0:T(8,128)(2,1)S(1)} %get-tuple-element.17), channel_id=1, source_target_pairs={{4,0},{6,2},{0,4},{2,6},{5,1},{7,3},{1,5},{3,7},{12,8},{14,10},{8,... | collective-permute-start | bytes 196616 | tf_op jit(solution)/shard_map/ppermute | solution.py:31
  32.8 0.2 collective-permute-done.3
  33.0 3.0 %collective-permute-done.4 = bf16[4,16,512]{2,1,0:T(8,128)(2,1)S(1)} collective-permute-done((bf16[4,16,512]{2,1,0:T(8,128)(2,1)S(1)}, bf16[4,16,512]{2,1,0:T(8,128)(2,1)S(1)}, u32[]{:S(2)}, u32[]{:S(2)}) %collective-permute-start.4) | collective-permute-done | bytes 65568 | tf_op jit(solution)/shard_map/ppermute | solution.py:31
  36.0 0.7 collective-permute-done.5
  36.9 11.5 %all-to-all-done = bf16[32,32,512]{2,1,0:T(8,128)(2,1)S(1)} async-done(((bf16[32,32,512]{2,1,0:T(8,128)(2,1)}), bf16[32,32,512]{2,1,0:T(8,128)(2,1)S(1)}, u32[]{:S(2)}, u32[]{:S(2)}) %all-to-all-start) | async-done | bytes 1048608 | tf_op jit(solution)/shard_map/all_to_all | solution.py:18
  48.4 0.9 fusion.33
  49.2 1.0 convolution_convert_fusion.3
  50.2 4.4 %all-to-all-start.1 = ((bf16[16,16,512]{2,1,0:T(8,128)(2,1)}), bf16[16,16,512]{2,1,0:T(8,128)(2,1)S(1)}, u32[]{:S(2)}, u32[]{:S(2)}) async-start(bf16[16,16,512]{2,1,0:T(8,128)(2,1)} %bitcast.20), calls=%async_computation.1 | async-start | bytes 524288 | tf_op jit(solution)/shard_map/all_to_all | solution.py:18
  54.9 7.3 %all-to-all-done.1 = bf16[16,16,512]{2,1,0:T(8,128)(2,1)S(1)} async-done(((bf16[16,16,512]{2,1,0:T(8,128)(2,1)}), bf16[16,16,512]{2,1,0:T(8,128)(2,1)S(1)}, u32[]{:S(2)}, u32[]{:S(2)}) %all-to-all-start.1) | async-done | bytes 262176 | tf_op jit(solution)/shard_map/all_to_all | solution.py:18
  62.7 2.8 %fusion.34 = f32[16,8,1,64]{3,2,1,0:T(1,128)S(1)} fusion(f32[16,8,64,1]{2,3,1,0:T(1,128)S(1)} %bitcast.98, f32[16,8,64,64]{3,2,1,0:T(8,128)} %param.22), kind=kOutput, calls=%fused_computation.116 | convolution fusion | flops 1048576 | bytes 2162688 | tf_op jit(solution)/shard_map/shd,shde->she/dot_general | solution.py:88
  65.5 0.2 multiply_reduce_fusion.1
  66.0 0.6 broadcast_in_dim.20
  66.6 3.3 %all-to-all-start.2 = ((bf16[4,16,512]{2,1,0:T(8,128)(2,1)}), bf16[4,16,512]{2,1,0:T(8,128)(2,1)S(1)}, u32[]{:S(2)}, u32[]{:S(2)}) async-start(bf16[4,16,512]{2,1,0:T(8,128)(2,1)} %broadcast_in_dim.20), calls=%async_computation.2 | async-start | bytes 131072 | tf_op jit(solution)/shard_map/all_to_all | solution.py:18
  70.0 4.3 %all-to-all-done.2 = bf16[4,16,512]{2,1,0:T(8,128)(2,1)S(1)} async-done(((bf16[4,16,512]{2,1,0:T(8,128)(2,1)}), bf16[4,16,512]{2,1,0:T(8,128)(2,1)S(1)}, u32[]{:S(2)}, u32[]{:S(2)}) %all-to-all-start.2) | async-done | bytes 65568 | tf_op jit(solution)/shard_map/all_to_all | solution.py:18
  74.3 1.3 convolution_convert_fusion.4
  75.7 0.7 broadcast_in_dim.22
  76.3 9.8 %all-to-all-start.3 = ((bf16[8,16,512]{2,1,0:T(8,128)(2,1)}), bf16[8,16,512]{2,1,0:T(8,128)(2,1)}, u32[]{:S(2)}, u32[]{:S(2)}) async-start(bf16[8,16,512]{2,1,0:T(8,128)(2,1)} %bitcast.31), calls=%async_computation.3 | async-start | bytes 262144 | tf_op jit(solution)/shard_map/all_to_all | solution.py:18
  86.2 1.3 pad_maximum_fusion
  87.5 4.0 %all-to-all-done.3 = bf16[8,16,512]{2,1,0:T(8,128)(2,1)} async-done(((bf16[8,16,512]{2,1,0:T(8,128)(2,1)}), bf16[8,16,512]{2,1,0:T(8,128)(2,1)}, u32[]{:S(2)}, u32[]{:S(2)}) %all-to-all-start.3) | async-done | bytes 131104 | tf_op jit(solution)/shard_map/all_to_all | solution.py:18
  91.5 1.1 reshape.226
  92.6 0.7 reduce_sum.102
  93.4 1.0 copy.38
  94.4 0.2 reshape.227
  94.7 0.9 fusion.14
  95.8 0.8 fusion.17
  96.6 1.5 fusion.35
  98.0 1.1 convolution_convert_fusion.2
  99.2 2.0 %reshape.228 = bf16[128,2,1024]{2,1,0:T(2,128)(2,1)} reshape(bf16[256,1024]{1,0:T(8,128)(2,1)} %convolution_convert_fusion.2) | data formatting | bytes 1048576 | tf_op jit(solution)/shard_map/reshape | solution.py:190
  101.2 7.3 %all-to-all-start.4 = ((bf16[128,2,1024]{2,1,0:T(2,128)(2,1)}), bf16[128,2,1024]{2,1,0:T(2,128)(2,1)}, u32[]{:S(2)}, u32[]{:S(2)}) async-start(bf16[128,2,1024]{2,1,0:T(2,128)(2,1)} %reshape.228), calls=%async_computation.4 | async-start | bytes 1048576 | tf_op jit(solution)/shard_map/all_to_all | solution.py:18
  108.5 1.5 fusion.5
  110.0 0.2 convolution_convert_fusion.5
  110.2 1.1 collective-permute-start.6
  111.3 4.3 %multiply_add_fusion = f32[16,8,64,64]{3,2,1,0:T(8,128)} fusion(f32[16,8,64,64]{3,2,1,0:T(8,128)} %param.22, f32[16,8,64]{2,1,0:T(8,128)S(1)} %reshape.234, f32[16,8,64]{2,1,0:T(8,128)S(1)} %get-tuple-element.44, f32[8]{0:T(128)S(1)} %copy-done.8), kind=kLoop, calls=%fused_computation.1 | loop fusion | flops 1572864 | bytes 4259872 | tf_op jit(solution)/shard_map/add | solution.py:92
  115.5 0.2 add_convert_fusion.1
  115.7 11.0 %all-to-all-done.4 = bf16[128,2,1024]{2,1,0:T(2,128)(2,1)} async-done(((bf16[128,2,1024]{2,1,0:T(2,128)(2,1)}), bf16[128,2,1024]{2,1,0:T(2,128)(2,1)}, u32[]{:S(2)}, u32[]{:S(2)}) %all-to-all-start.4) | async-done | bytes 524320 | tf_op jit(solution)/shard_map/all_to_all | solution.py:18
  126.8 2.0 %reshape.229 = bf16[256,1024]{1,0:T(8,128)(2,1)} reshape(bf16[128,2,1024]{2,1,0:T(2,128)(2,1)} %all-to-all-done.4) | data formatting | bytes 1048576 | tf_op jit(solution)/shard_map/reshape | solution.py:221
  128.8 3.0 %collective-permute-start.7 = (bf16[256,1024]{1,0:T(8,128)(2,1)}, bf16[256,1024]{1,0:T(8,128)(2,1)S(1)}, u32[]{:S(2)}, u32[]{:S(2)}) collective-permute-start(bf16[256,1024]{1,0:T(8,128)(2,1)} %reshape.229), channel_id=1, source_target_pairs={{0,1},{1,0},{2,3},{3,2},{4,5},{5,4},{6,7},{7,6},{8,9},{9,8},{10,11... | collective-permute-start | bytes 1572872 | tf_op jit(solution)/shard_map/ppermute | solution.py:26
  131.8 1.5 fusion.36
  133.3 0.3 collective-permute-done.7
  133.5 0.4 convolution_add_fusion
  134.1 0.3 convolution_convert_fusion
  134.4 0.5 collective-permute-start.8
  134.9 1.5 collective-permute-done.8
  136.4 0.3 add_convert_fusion
  136.7 1.0 reshape.230
  137.7 6.2 %all-to-all-start.5 = ((bf16[128,2,1024]{2,1,0:T(2,128)(2,1)}), bf16[128,2,1024]{2,1,0:T(2,128)(2,1)S(1)}, u32[]{:S(2)}, u32[]{:S(2)}) async-start(bf16[128,2,1024]{2,1,0:T(2,128)(2,1)} %reshape.230), calls=%async_computation.5 | async-start | bytes 1048576 | tf_op jit(solution)/shard_map/all_to_all | solution.py:18
  144.0 19.1 %all-to-all-done.5 = bf16[128,2,1024]{2,1,0:T(2,128)(2,1)S(1)} async-done(((bf16[128,2,1024]{2,1,0:T(2,128)(2,1)}), bf16[128,2,1024]{2,1,0:T(2,128)(2,1)S(1)}, u32[]{:S(2)}, u32[]{:S(2)}) %all-to-all-start.5) | async-done | bytes 524320 | tf_op jit(solution)/shard_map/all_to_all | solution.py:18
  163.1 0.2 reshape.231
  163.3 0.2 convolution_add_fusion.1
  163.5 2.5 %collective-permute-start.9 = (f32[16,1024]{1,0:T(8,128)S(1)}, f32[16,1024]{1,0:T(8,128)S(1)}, u32[]{:S(2)}, u32[]{:S(2)}) collective-permute-start(f32[16,1024]{1,0:T(8,128)S(1)} %convolution_add_fusion.1), channel_id=1, source_target_pairs={{0,1},{1,0},{2,3},{3,2},{4,5},{5,4},{6,7},{7,6},{8,9},{9,8},{10,11... | collective-permute-start | bytes 196616 | tf_op jit(solution)/shard_map/ppermute | solution.py:26
  166.0 0.9 collective-permute-done.9
  167.0 0.7 fusion.18
  (81 shorter events, 3.0 us)
Async XLA Ops:
  0.6 109.4 %copy-start = (bf16[256,2048]{1,0:T(8,128)(2,1)S(1)}, bf16[256,2048]{1,0:T(8,128)(2,1)}, u32[]{:S(2)}) copy-start(bf16[256,2048]{1,0:T(8,128)(2,1)} %param.39) | copy-start | bytes 3145732
  0.6 22.0 %copy-start.3 = (s32[16,6]{0,1:T(8,128)S(1)}, s32[16,6]{0,1:T(8,128)}, u32[]{:S(2)}) copy-start(s32[16,6]{0,1:T(8,128)} %param.32) | copy-start | bytes 1156
  3.1 25.3 %collective-permute-start.2 = (bf16[16,512]{1,0:T(8,128)(2,1)S(1)}, bf16[16,512]{1,0:T(8,128)(2,1)S(1)}, u32[]{:S(2)}, u32[]{:S(2)}) collective-permute-start(bf16[16,512]{1,0:T(8,128)(2,1)S(1)} %get-tuple-element.33), channel_id=1, source_target_pairs={{24,0},{0,8},{8,16},{16,24},{25,1},{1,9},{9,17},{17,25},{26,2},{2,... | collective-permute-start | bytes 49160 | tf_op jit(solution)/shard_map/ppermute | solution.py:31
  5.3 23.1 %collective-permute-start.1 = (bf16[16,512]{1,0:T(8,128)(2,1)S(1)}, bf16[16,512]{1,0:T(8,128)(2,1)S(1)}, u32[]{:S(2)}, u32[]{:S(2)}) collective-permute-start(bf16[16,512]{1,0:T(8,128)(2,1)S(1)} %get-tuple-element.35), channel_id=1, source_target_pairs={{16,0},{24,8},{0,16},{8,24},{17,1},{25,9},{1,17},{9,25},{18,2},{26... | collective-permute-start | bytes 49160 | tf_op jit(solution)/shard_map/ppermute | solution.py:31
  7.9 20.4 %collective-permute-start = (bf16[16,512]{1,0:T(8,128)(2,1)S(1)}, bf16[16,512]{1,0:T(8,128)(2,1)S(1)}, u32[]{:S(2)}, u32[]{:S(2)}) collective-permute-start(bf16[16,512]{1,0:T(8,128)(2,1)S(1)} %get-tuple-element.36), channel_id=1, source_target_pairs={{8,0},{16,8},{24,16},{0,24},{9,1},{17,9},{25,17},{1,25},{10,2},{18... | collective-permute-start | bytes 49160 | tf_op jit(solution)/shard_map/ppermute | solution.py:31
  11.6 36.8 %all-to-all-start = ((bf16[32,32,512]{2,1,0:T(8,128)(2,1)}), bf16[32,32,512]{2,1,0:T(8,128)(2,1)S(1)}, u32[]{:S(2)}, u32[]{:S(2)}) async-start(bf16[32,32,512]{2,1,0:T(8,128)(2,1)} %bitcast.18), calls=%async_computation | async-start | bytes 2097152 | tf_op jit(solution)/shard_map/all_to_all | solution.py:18
  26.1 28.6 %copy-start.9 = (s32[16]{0:T(128)S(1)}, s32[16]{0:T(128)}, u32[]{:S(2)}) copy-start(s32[16]{0:T(128)} %param.21) | copy-start | bytes 196
  28.5 4.5 %collective-permute-start.3 = (bf16[4,16,512]{2,1,0:T(8,128)(2,1)S(1)}, bf16[4,16,512]{2,1,0:T(8,128)(2,1)S(1)}, u32[]{:S(2)}, u32[]{:S(2)}) collective-permute-start(bf16[4,16,512]{2,1,0:T(8,128)(2,1)S(1)} %get-tuple-element.17), channel_id=1, source_target_pairs={{2,0},{4,2},{6,4},{0,6},{3,1},{5,3},{7,5},{1,7},{10,8},{12,10},{14... | collective-permute-start | bytes 196616 | tf_op jit(solution)/shard_map/ppermute | solution.py:31
  31.0 5.8 %collective-permute-start.5 = (bf16[4,16,512]{2,1,0:T(8,128)(2,1)S(1)}, bf16[4,16,512]{2,1,0:T(8,128)(2,1)S(1)}, u32[]{:S(2)}, u32[]{:S(2)}) collective-permute-start(bf16[4,16,512]{2,1,0:T(8,128)(2,1)S(1)} %get-tuple-element.17), channel_id=1, source_target_pairs={{6,0},{0,2},{2,4},{4,6},{7,1},{1,3},{3,5},{5,7},{14,8},{8,10},{10,... | collective-permute-start | bytes 196616 | tf_op jit(solution)/shard_map/ppermute | solution.py:31
  31.1 4.9 %collective-permute-start.4 = (bf16[4,16,512]{2,1,0:T(8,128)(2,1)S(1)}, bf16[4,16,512]{2,1,0:T(8,128)(2,1)S(1)}, u32[]{:S(2)}, u32[]{:S(2)}) collective-permute-start(bf16[4,16,512]{2,1,0:T(8,128)(2,1)S(1)} %get-tuple-element.17), channel_id=1, source_target_pairs={{4,0},{6,2},{0,4},{2,6},{5,1},{7,3},{1,5},{3,7},{12,8},{14,10},{8,... | collective-permute-start | bytes 196616 | tf_op jit(solution)/shard_map/ppermute | solution.py:31
  50.2 12.0 %all-to-all-start.1 = ((bf16[16,16,512]{2,1,0:T(8,128)(2,1)}), bf16[16,16,512]{2,1,0:T(8,128)(2,1)S(1)}, u32[]{:S(2)}, u32[]{:S(2)}) async-start(bf16[16,16,512]{2,1,0:T(8,128)(2,1)} %bitcast.20), calls=%async_computation.1 | async-start | bytes 524288 | tf_op jit(solution)/shard_map/all_to_all | solution.py:18
  54.8 15.2 %copy-start.7 = (f32[8]{0:T(128)}, f32[8]{0:T(128)S(1)}, u32[]{:S(2)}) copy-start(f32[8]{0:T(128)S(1)} %dynamic_slice.61) | copy-start | bytes 100
  65.5 29.2 %copy-start.4 = (f32[2048]{0:T(1024)S(1)}, f32[2048]{0:T(1024)}, u32[]{:S(2)}) copy-start(f32[2048]{0:T(1024)} %param.24) | copy-start | bytes 24580
  66.6 7.7 %all-to-all-start.2 = ((bf16[4,16,512]{2,1,0:T(8,128)(2,1)}), bf16[4,16,512]{2,1,0:T(8,128)(2,1)S(1)}, u32[]{:S(2)}, u32[]{:S(2)}) async-start(bf16[4,16,512]{2,1,0:T(8,128)(2,1)} %broadcast_in_dim.20), calls=%async_computation.2 | async-start | bytes 131072 | tf_op jit(solution)/shard_map/all_to_all | solution.py:18
  76.3 15.2 %all-to-all-start.3 = ((bf16[8,16,512]{2,1,0:T(8,128)(2,1)}), bf16[8,16,512]{2,1,0:T(8,128)(2,1)}, u32[]{:S(2)}, u32[]{:S(2)}) async-start(bf16[8,16,512]{2,1,0:T(8,128)(2,1)} %bitcast.31), calls=%async_computation.3 | async-start | bytes 262144 | tf_op jit(solution)/shard_map/all_to_all | solution.py:18
  94.6 16.7 %copy-start.8 = (f32[8]{0:T(128)S(1)}, f32[8]{0:T(128)}, u32[]{:S(2)}) copy-start(f32[8]{0:T(128)} %copy-done.7) | copy-start | bytes 100
  101.2 25.5 %all-to-all-start.4 = ((bf16[128,2,1024]{2,1,0:T(2,128)(2,1)}), bf16[128,2,1024]{2,1,0:T(2,128)(2,1)}, u32[]{:S(2)}, u32[]{:S(2)}) async-start(bf16[128,2,1024]{2,1,0:T(2,128)(2,1)} %reshape.228), calls=%async_computation.4 | async-start | bytes 1048576 | tf_op jit(solution)/shard_map/all_to_all | solution.py:18
  110.2 5.3 %collective-permute-start.6 = (bf16[16,1024]{1,0:T(8,128)(2,1)S(1)}, bf16[16,1024]{1,0:T(8,128)(2,1)S(1)}, u32[]{:S(2)}, u32[]{:S(2)}) collective-permute-start(bf16[16,1024]{1,0:T(8,128)(2,1)S(1)} %convolution_convert_fusion.5), channel_id=1, source_target_pairs={{0,1},{1,0},{2,3},{3,2},{4,5},{5,4},{6,7},{7,6},{8,9},{9,8},{10,11... | collective-permute-start | bytes 98312 | tf_op jit(solution)/shard_map/ppermute | solution.py:26
  128.8 5.3 %copy-start.2 = (bf16[256,1024]{1,0:T(8,128)(2,1)S(1)}, bf16[256,1024]{1,0:T(8,128)(2,1)}, u32[]{:S(2)}) copy-start(bf16[256,1024]{1,0:T(8,128)(2,1)} %get-tuple-element.14) | copy-start | bytes 1572868
  128.8 7.6 %copy-start.1 = (bf16[256,1024]{1,0:T(8,128)(2,1)S(1)}, bf16[256,1024]{1,0:T(8,128)(2,1)}, u32[]{:S(2)}) copy-start(bf16[256,1024]{1,0:T(8,128)(2,1)} %get-tuple-element.13) | copy-start | bytes 1572868
  128.8 4.7 %collective-permute-start.7 = (bf16[256,1024]{1,0:T(8,128)(2,1)}, bf16[256,1024]{1,0:T(8,128)(2,1)S(1)}, u32[]{:S(2)}, u32[]{:S(2)}) collective-permute-start(bf16[256,1024]{1,0:T(8,128)(2,1)} %reshape.229), channel_id=1, source_target_pairs={{0,1},{1,0},{2,3},{3,2},{4,5},{5,4},{6,7},{7,6},{8,9},{9,8},{10,11... | collective-permute-start | bytes 1572872 | tf_op jit(solution)/shard_map/ppermute | solution.py:26
  133.3 10.6 %copy-start.6 = (f32[16,6]{0,1:T(8,128)S(1)}, f32[16,6]{0,1:T(8,128)}, u32[]{:S(2)}) copy-start(f32[16,6]{0,1:T(8,128)} %param.33) | copy-start | bytes 1156
  134.0 33.0 %copy-start.5 = (f32[2048]{0:T(1024)S(1)}, f32[2048]{0:T(1024)}, u32[]{:S(2)}) copy-start(f32[2048]{0:T(1024)} %param.26) | copy-start | bytes 24580
  134.4 2.0 %collective-permute-start.8 = (bf16[256,1024]{1,0:T(8,128)(2,1)S(1)}, bf16[256,1024]{1,0:T(8,128)(2,1)S(1)}, u32[]{:S(2)}, u32[]{:S(2)}) collective-permute-start(bf16[256,1024]{1,0:T(8,128)(2,1)S(1)} %convolution_convert_fusion), channel_id=1, source_target_pairs={{0,1},{1,0},{2,3},{3,2},{4,5},{5,4},{6,7},{7,6},{8,9},{9,8},{10,11... | collective-permute-start | bytes 1572872 | tf_op jit(solution)/shard_map/ppermute | solution.py:26
  137.7 25.4 %all-to-all-start.5 = ((bf16[128,2,1024]{2,1,0:T(2,128)(2,1)}), bf16[128,2,1024]{2,1,0:T(2,128)(2,1)S(1)}, u32[]{:S(2)}, u32[]{:S(2)}) async-start(bf16[128,2,1024]{2,1,0:T(2,128)(2,1)} %reshape.230), calls=%async_computation.5 | async-start | bytes 1048576 | tf_op jit(solution)/shard_map/all_to_all | solution.py:18
  163.5 3.4 %collective-permute-start.9 = (f32[16,1024]{1,0:T(8,128)S(1)}, f32[16,1024]{1,0:T(8,128)S(1)}, u32[]{:S(2)}, u32[]{:S(2)}) collective-permute-start(f32[16,1024]{1,0:T(8,128)S(1)} %convolution_add_fusion.1), channel_id=1, source_target_pairs={{0,1},{1,0},{2,3},{3,2},{4,5},{5,4},{6,7},{7,6},{8,9},{9,8},{10,11... | collective-permute-start | bytes 196616 | tf_op jit(solution)/shard_map/ppermute | solution.py:26

commit v3 on v2

--- a/solution.py
+++ b/solution.py
@@ -24,6 +24,11 @@
 
 def from_partner(value):
     return lax.ppermute(value, "tp", [(0, 1), (1, 0)])
+
+
+def rolled_lanes(rows, start):
+    doubled = jnp.concatenate([rows, rows], axis=1)
+    return lax.dynamic_slice_in_dim(doubled, start, rows.shape[1], 1)
 
 
 def from_ahead(value, axis, step):
@@ -88,15 +93,18 @@
     from_state = jnp.einsum("shd,shde->she", rot_query, prior_state)
     self_term = jnp.sum(rot_query * rot_key, axis=-1, keepdims=True)
     read_out = decays[None, :, None] * from_state + self_term * wide_values
-    new_state = (
-        decays[None, :, None, None] * prior_state
-        + rot_key[..., :, None] * wide_values[..., None, :]
-    )
     normed = read_out * lax.rsqrt(jnp.mean(read_out * read_out, axis=-1, keepdims=True) + EPS)
     gated_rows = normed.reshape(seq_count, head_count * HEAD) * jax.nn.silu(
         out_gate.astype(jnp.float32)
     )
-    return (gated_rows.astype(jnp.bfloat16), new_state)
+    return (gated_rows.astype(jnp.bfloat16), rot_key, wide_values)
+
+
+def next_state(decays, prior_state, rot_key, wide_values):
+    return (
+        decays[None, :, None, None] * prior_state
+        + rot_key[..., :, None] * wide_values[..., None, :]
+    )
 
 
 def on_device(
@@ -127,15 +135,17 @@
     experts_all = depth * rows_y * rows_x
     plane = rows_y * rows_x
     core = lax.axis_index("tp")
-    half = width // 2
 
     kinds = jnp.stack([query_weight, key_weight, value_weight, gate_weight])
-    wout_rows = copies(out_weight.T, rows_x)
-    sent = copies(jnp.concatenate([kinds, wout_rows], axis=1), depth)
-    held = exchanged(sent.reshape(depth * rows_x, -1, cols), (Z, X))
-    kind_rows = query_weight.shape[0]
-    kind_weight = held[:, :kind_rows].reshape(-1, cols)
-    wout_zx = held[:, kind_rows:].reshape(-1, cols)
+    share = cols // rows_x
+    wout_parts = out_weight.reshape(rows_x, share, -1).swapaxes(1, 2)
+    sent = copies(jnp.concatenate([kinds, wout_parts], axis=2), depth)
+    held = exchanged(sent.reshape(depth * rows_x, -1, cols + share), (Z, X))
+    held = held.reshape(-1, cols + share)
+    kind_weight = held[:, :cols]
+    wout_part = held[:, cols:]
+    others = [from_ahead(wout_part, X, step) for step in range(1, rows_x)]
+    wout_turned = jnp.concatenate([wout_part, *others], axis=1)
 
     normed = scaled_rows(tokens, mix_gain).astype(jnp.bfloat16)
     by_y = normed.reshape(seq_here, depth, rows_y, -1).transpose(2, 0, 1, 3)
@@ -149,11 +159,14 @@
 
     heads_here = cols // HEAD
     decays = lax.dynamic_slice_in_dim(decay_table(HEADS), core * heads_here, heads_here, 0)
-    retained, new_state = retain(queries, keys_new, values, out_gate, prior_state, lengths, decays)
-
-    retained_y = exchanged(copies(retained, rows_y), Y).reshape(rows_y * seq_here, cols)
+    retained, rot_key, wide_values = retain(
+        queries, keys_new, values, out_gate, prior_state, lengths, decays
+    )
+
+    turned = rolled_lanes(retained, lax.axis_index(X) * share)
+    retained_y = exchanged(copies(turned, rows_y), Y).reshape(rows_y * seq_here, cols)
     partial_mix = lax.dot_general(
-        retained_y, wout_zx, (((1,), (1,)), ((), ())), preferred_element_type=jnp.float32
+        retained_y, wout_turned, (((1,), (1,)), ((), ())), preferred_element_type=jnp.float32
     ).astype(jnp.bfloat16)
     to_both = partial_mix.reshape(rows_y, 1, seq_here, -1)
     to_both = jnp.broadcast_to(to_both, (rows_y, 2, *to_both.shape[2:]))
@@ -165,78 +178,53 @@
     middle = rounded(tokens.astype(jnp.float32) + scaled_rows(mixed_sum, post_gain))
     moe_in = scaled_rows(middle, ffn_gain).astype(jnp.bfloat16)
 
-    topk_here = routes.shape[1]
-    capacity = seq_here * topk_here // experts_all + 2
-    slot_count = experts_all * capacity
     flat_routes = routes.reshape(-1)
     onehot = (flat_routes[:, None] == jnp.arange(experts_all, dtype=jnp.int32)[None, :]).astype(
         jnp.int32
     )
     earlier = jnp.cumsum(onehot, axis=0) - onehot
     ranks = jnp.sum(earlier * onehot, axis=1)
-    slot_ids = flat_routes * capacity + ranks
-    placing = (jnp.arange(slot_count, dtype=jnp.int32)[:, None] == slot_ids[None, :]).reshape(
-        slot_count, seq_here, topk_here
+    mine = jnp.where(ranks == core, flat_routes, -1)
+    placing = (jnp.arange(experts_all, dtype=jnp.int32)[:, None] == mine[None, :]).reshape(
+        experts_all, seq_here, -1
     )
     dispatch_rows = jnp.any(placing, axis=2).astype(jnp.bfloat16)
     combine = jnp.sum(
         jnp.where(placing, route_gates[None, :, :], jnp.zeros((), jnp.float32)), axis=2
     ).T
 
-    moe_half = lax.dynamic_slice_in_dim(moe_in, core * half, half, 1)
-    outgoing = jnp.dot(dispatch_rows, moe_half, preferred_element_type=jnp.float32).astype(
+    outgoing = jnp.dot(dispatch_rows, moe_in, preferred_element_type=jnp.float32).astype(
         jnp.bfloat16
     )
-    arrived = exchanged(outgoing.reshape(experts_all, capacity, half), EP)
-    own_at, other_at = core * half, (1 - core) * half
-
-    def down_halves(weight):
-        return tuple(lax.dynamic_slice_in_dim(weight, at, half, 1) for at in (own_at, other_at))
-
-    def up_halves():
-        both = (expert_gate[0], expert_up[0])
-        return tuple(
-            jnp.concatenate([lax.dynamic_slice_in_dim(w, at, half, 0) for w in both], axis=1)
-            for at in (own_at, other_at)
-        )
-
-    def summed_half(rows, halves):
-        kept, sent = (
-            jnp.dot(rows, piece, preferred_element_type=jnp.float32).astype(jnp.bfloat16)
-            for piece in halves
-        )
-        got = from_partner(sent)
-        return (kept.astype(jnp.float32) + got.astype(jnp.float32)).astype(jnp.bfloat16)
-
-    shared_hidden = (
-        jax.nn.silu(jnp.dot(moe_in, shared_gate, preferred_element_type=jnp.float32))
-        * jnp.dot(moe_in, shared_up, preferred_element_type=jnp.float32)
-    ).astype(jnp.bfloat16)
-    shared_out = summed_half(shared_hidden, down_halves(shared_down))
-
-    beside = (shared_out, new_state, up_halves(), down_halves(expert_down[0]))
-    arrived, beside = lax.optimization_barrier((arrived, beside))
-    shared_out, new_state, up_pieces, down_pieces = beside
-
-    own_in = arrived.reshape(slot_count, half)
+    outgoing, moe_beside, state_beside = lax.optimization_barrier((outgoing, moe_in, prior_state))
+    arrived = exchanged(outgoing.reshape(experts_all, 2, -1), EP)
+
+    def lifted(rows, w_gate, w_up):
+        return (
+            jax.nn.silu(jnp.dot(rows, w_gate, preferred_element_type=jnp.float32))
+            * jnp.dot(rows, w_up, preferred_element_type=jnp.float32)
+        ).astype(jnp.bfloat16)
+
+    def lowered(rows, w_down):
+        return jnp.dot(rows, w_down, preferred_element_type=jnp.float32).astype(jnp.bfloat16)
+
+    new_state = next_state(decays, state_beside, rot_key, wide_values)
+    shared_part = lowered(lifted(moe_beside, shared_gate, shared_up), shared_down)
+    arrived, shared_part, new_state = lax.optimization_barrier((arrived, shared_part, new_state))
+
+    own_in = arrived.reshape(experts_all, width)
     other_in = from_partner(own_in)
-    lifted = jnp.dot(own_in, up_pieces[0], preferred_element_type=jnp.float32) + jnp.dot(
-        other_in, up_pieces[1], preferred_element_type=jnp.float32
-    )
-    gate_part, up_part = jnp.split(lifted, 2, axis=1)
-    hidden = (jax.nn.silu(gate_part) * up_part).astype(jnp.bfloat16)
-    expert_sum = summed_half(hidden, down_pieces)
-    returned = exchanged(expert_sum.reshape(experts_all, capacity, half), EP)
-    back_rows = returned.reshape(slot_count, half).astype(jnp.float32)
-    routed = jnp.dot(combine, back_rows)
-    mixture = shared_out.astype(jnp.float32) + routed
-    other_mixture = from_partner(mixture)
-    whole = jnp.where(
-        core == 0,
-        jnp.concatenate([mixture, other_mixture], axis=1),
-        jnp.concatenate([other_mixture, mixture], axis=1),
-    )
-    result = (middle + scaled_rows(whole, out_gain)).astype(jnp.bfloat16)
+    own_hidden = lifted(own_in, expert_gate[0], expert_up[0])
+    own_hidden, other_in = lax.optimization_barrier((own_hidden, other_in))
+    other_hidden = lifted(other_in, expert_gate[0], expert_up[0])
+    got = from_partner(lowered(other_hidden, expert_down[0]))
+    own_sum = lowered(own_hidden, expert_down[0]).astype(jnp.float32) + got.astype(jnp.float32)
+    own_sum = own_sum.astype(jnp.bfloat16)
+    returned = exchanged(own_sum.reshape(experts_all, 2, -1), EP)
+    back_rows = returned.reshape(experts_all, width).astype(jnp.float32)
+    mixture_part = jnp.dot(combine, back_rows) + shared_part.astype(jnp.float32)
+    mixture = mixture_part + from_partner(mixture_part)
+    result = (middle + scaled_rows(mixture, out_gain)).astype(jnp.bfloat16)
     return (result, new_state)
 
 

time: 169 us -> 150 us (0.89)
  local copies, waits for them, and re-layouts: 17.8 us -> 7.91 us
  waiting for transfers between devices: 63.9 us -> 56 us
  other arithmetic: 13.3 us -> 9.85 us
  starting transfers between devices: 59.3 us -> 61.8 us
    all_to_all x6, waiting for transfers between devices: 57.2 us -> 48.9 us  [exchanged(): return lax.all_to_all(blocks, axes, split_axis=0, concat_axis=0, tiled=True)]
    ppermute x6 -> x9, starting transfers between devices: 10.2 us -> 15.2 us  [from_ahead(): lax.ppermute(value, axis, [((i + step) % size, i) for i in range(size)])]
    dynamic_slice x2 -> x0, local copies, waits for them, and re-layouts: 4.95 us -> none  [the longest x1 2.7 us: up_halves(): lax.dynamic_slice_in_dim(w, at, half, 0)]
    reshape x4 -> x2, local copies, waits for them, and re-layouts: 5.27 us -> 2.33 us  [the longest x1 1.16 us: on_device(): arrived = exchanged(outgoing.reshape(experts_all, 2, -1), EP)]
    ppermute x4 -> x3, starting transfers between devices: 7.02 us -> 5.54 us  [from_partner(): return lax.ppermute(value, 'tp', [(0, 1), (1, 0)])]
    dot_general x11 -> x10, matrix products: 8.48 us -> 7.83 us  [the longest x3 3.37 us: lowered(): jnp.dot(rows, w_down, preferred_element_type=jnp.float32)]
    ppermute x6 -> x9, waiting for transfers between devices: 3.92 us -> 4.22 us  [from_ahead(): lax.ppermute(value, axis, [((i + step) % size, i) for i in range(size)])]
    add x2 -> x1, other arithmetic: 4.27 us -> 4.37 us  [next_state(): decays[None, :, None, None] * prior_state]
  transfers between devices with their start and end apart: 16 -> 18, of which waited for: 12 -> 10; matrix products, arithmetic and copies ran while one was open for 11% -> 13% of each run, Pallas kernels for 0% -> 0%
where the time goes in v3:
time: 150 us; the launch traced here: 149 us
  starting transfers between devices  61.8 us (41%)
  waiting for transfers between devices  56 us (37%)
  matrix products  11.7 us (8%)
  other arithmetic  9.85 us (7%)
  local copies, waits for them, and re-layouts  7.91 us (5%)
    all_to_all x6, waiting for transfers between devices, exchanged(): return lax.all_to_all(blocks, axes, split_axis=0, concat_axis=0, tiled=True)  48.9 us
    all_to_all x6, starting transfers between devices, exchanged(): return lax.all_to_all(blocks, axes, split_axis=0, concat_axis=0, tiled=True)  41 us
    ppermute x9, starting transfers between devices, from_ahead(): lax.ppermute(value, axis, [((i + step) % size, i) for i in range(size)])  15.2 us
    ppermute x3, starting transfers between devices, from_partner(): return lax.ppermute(value, 'tp', [(0, 1), (1, 0)])  5.54 us
    add x1, other arithmetic, next_state(): decays[None, :, None, None] * prior_state  4.37 us
    ppermute x9, waiting for transfers between devices, from_ahead(): lax.ppermute(value, axis, [((i + step) % size, i) for i in range(size)])  4.22 us
    dot_general x3, matrix products, lowered(): jnp.dot(rows, w_down, preferred_element_type=jnp.float32)  3.37 us
  transfers between devices with their start and end apart: 18, of which 10 were waited for; matrix products, arithmetic and copies ran while one was open for 13% of the time, Pallas kernels for 0%

profile of v3, /device:TPU:1, one launch (start us, length us, event | category | flops | bytes accessed | tf_op | source)
XLA Modules:
  0.0 148.6 jit_solution(5279484377652044129)
XLA Ops:
  0.7 1.0 fusion.27
  1.8 0.9 fusion.29
  2.7 0.2 reshape.211
  2.9 0.1 reshape.212
  3.1 2.2 %collective-permute-start.2 = (bf16[16,512]{1,0:T(8,128)(2,1)S(1)}, bf16[16,512]{1,0:T(8,128)(2,1)S(1)}, u32[]{:S(2)}, u32[]{:S(2)}) collective-permute-start(bf16[16,512]{1,0:T(8,128)(2,1)S(1)} %get-tuple-element.29), channel_id=1, source_target_pairs={{24,0},{0,8},{8,16},{16,24},{25,1},{1,9},{9,17},{17,25},{26,2},{2,... | collective-permute-start | bytes 49160 | tf_op jit(solution)/shard_map/ppermute | solution.py:36
  5.3 2.6 %collective-permute-start.1 = (bf16[16,512]{1,0:T(8,128)(2,1)S(1)}, bf16[16,512]{1,0:T(8,128)(2,1)S(1)}, u32[]{:S(2)}, u32[]{:S(2)}) collective-permute-start(bf16[16,512]{1,0:T(8,128)(2,1)S(1)} %get-tuple-element.31), channel_id=1, source_target_pairs={{16,0},{24,8},{0,16},{8,24},{17,1},{25,9},{1,17},{9,25},{18,2},{26... | collective-permute-start | bytes 49160 | tf_op jit(solution)/shard_map/ppermute | solution.py:36
  7.9 1.1 collective-permute-start
  9.0 0.7 bitcast_bitcast_fusion
  9.7 0.8 pad_maximum_fusion
  10.5 0.9 broadcast_in_dim.19
  11.4 11.0 %all-to-all-start = ((bf16[32,16,640]{2,1,0:T(8,128)(2,1)}), bf16[32,16,640]{2,1,0:T(8,128)(2,1)S(1)}, u32[]{:S(2)}, u32[]{:S(2)}) async-start(bf16[32,16,640]{2,1,0:T(8,128)(2,1)} %bitcast.18), calls=%async_computation | async-start | bytes 1310720 | tf_op jit(solution)/shard_map/all_to_all | solution.py:18
  22.4 0.8 copy.36
  23.4 0.1 reduce_window_sum.11
  23.5 0.2 select_reduce_fusion.1
  23.9 2.5 %collective-permute-start.3 = (bf16[4,16,512]{2,1,0:T(8,128)(2,1)S(1)}, bf16[4,16,512]{2,1,0:T(8,128)(2,1)S(1)}, u32[]{:S(2)}, u32[]{:S(2)}) collective-permute-start(bf16[4,16,512]{2,1,0:T(8,128)(2,1)S(1)} %get-tuple-element.21), channel_id=1, source_target_pairs={{2,0},{4,2},{6,4},{0,6},{3,1},{5,3},{7,5},{1,7},{10,8},{12,10},{14... | collective-permute-start | bytes 196616 | tf_op jit(solution)/shard_map/ppermute | solution.py:36
  26.5 1.7 %collective-permute-start.4 = (bf16[4,16,512]{2,1,0:T(8,128)(2,1)S(1)}, bf16[4,16,512]{2,1,0:T(8,128)(2,1)S(1)}, u32[]{:S(2)}, u32[]{:S(2)}) collective-permute-start(bf16[4,16,512]{2,1,0:T(8,128)(2,1)S(1)} %get-tuple-element.21), channel_id=1, source_target_pairs={{4,0},{6,2},{0,4},{2,6},{5,1},{7,3},{1,5},{3,7},{12,8},{14,10},{8,... | collective-permute-start | bytes 196616 | tf_op jit(solution)/shard_map/ppermute | solution.py:36
  28.2 3.5 %collective-permute-done.4 = bf16[4,16,512]{2,1,0:T(8,128)(2,1)S(1)} collective-permute-done((bf16[4,16,512]{2,1,0:T(8,128)(2,1)S(1)}, bf16[4,16,512]{2,1,0:T(8,128)(2,1)S(1)}, u32[]{:S(2)}, u32[]{:S(2)}) %collective-permute-start.4) | collective-permute-done | bytes 65568 | tf_op jit(solution)/shard_map/ppermute | solution.py:36
  31.7 0.7 collective-permute-done.5
  32.6 7.5 %all-to-all-done = bf16[32,16,640]{2,1,0:T(8,128)(2,1)S(1)} async-done(((bf16[32,16,640]{2,1,0:T(8,128)(2,1)}), bf16[32,16,640]{2,1,0:T(8,128)(2,1)S(1)}, u32[]{:S(2)}, u32[]{:S(2)}) %all-to-all-start) | async-done | bytes 655392 | tf_op jit(solution)/shard_map/all_to_all | solution.py:18
  40.0 1.0 convolution_convert_fusion.4
  41.0 4.8 %all-to-all-start.1 = ((bf16[16,16,512]{2,1,0:T(8,128)(2,1)}), bf16[16,16,512]{2,1,0:T(8,128)(2,1)S(1)}, u32[]{:S(2)}, u32[]{:S(2)}) async-start(bf16[16,16,512]{2,1,0:T(8,128)(2,1)} %bitcast.20), calls=%async_computation.1 | async-start | bytes 524288 | tf_op jit(solution)/shard_map/all_to_all | solution.py:18
  46.0 0.1 multiply_cosine_fusion
  46.1 1.4 collective-permute-start.8
  47.5 2.4 %collective-permute-start.7 = (bf16[512,128]{1,0:T(8,128)(2,1)S(1)}, bf16[512,128]{1,0:T(8,128)(2,1)S(1)}, u32[]{:S(2)}, u32[]{:S(2)}) collective-permute-start(bf16[512,128]{1,0:T(8,128)(2,1)S(1)} %slice.29), channel_id=1, source_target_pairs={{4,0},{6,2},{0,4},{2,6},{5,1},{7,3},{1,5},{3,7},{12,8},{14,10},{8,... | collective-permute-start | bytes 393224 | tf_op jit(solution)/shard_map/ppermute | solution.py:36
  49.9 1.2 collective-permute-start.6
  51.1 2.3 %all-to-all-done.1 = bf16[16,16,512]{2,1,0:T(8,128)(2,1)S(1)} async-done(((bf16[16,16,512]{2,1,0:T(8,128)(2,1)}), bf16[16,16,512]{2,1,0:T(8,128)(2,1)S(1)}, u32[]{:S(2)}, u32[]{:S(2)}) %all-to-all-start.1) | async-done | bytes 262176 | tf_op jit(solution)/shard_map/all_to_all | solution.py:18
  53.9 2.9 %fusion.58 = f32[16,8,1,64]{3,2,1,0:T(1,128)S(1)} fusion(f32[16,8,64,1]{2,3,1,0:T(1,128)S(1)} %bitcast.114, f32[16,8,64,64]{3,2,1,0:T(8,128)} %param.22), kind=kOutput, calls=%fused_computation.130 | convolution fusion | flops 1048576 | bytes 2162688 | tf_op jit(solution)/shard_map/shd,shde->she/dot_general | solution.py:93
  56.8 0.2 multiply_reduce_fusion.1
  57.3 0.6 broadcast_in_dim.20
  57.9 3.3 %all-to-all-start.2 = ((bf16[4,16,512]{2,1,0:T(8,128)(2,1)}), bf16[4,16,512]{2,1,0:T(8,128)(2,1)S(1)}, u32[]{:S(2)}, u32[]{:S(2)}) async-start(bf16[4,16,512]{2,1,0:T(8,128)(2,1)} %broadcast_in_dim.20), calls=%async_computation.2 | async-start | bytes 131072 | tf_op jit(solution)/shard_map/all_to_all | solution.py:18
  61.4 4.3 %all-to-all-done.2 = bf16[4,16,512]{2,1,0:T(8,128)(2,1)S(1)} async-done(((bf16[4,16,512]{2,1,0:T(8,128)(2,1)}), bf16[4,16,512]{2,1,0:T(8,128)(2,1)S(1)}, u32[]{:S(2)}, u32[]{:S(2)}) %all-to-all-start.2) | async-done | bytes 65568 | tf_op jit(solution)/shard_map/all_to_all | solution.py:18
  65.7 0.3 convolution_convert_fusion.5
  65.9 0.7 broadcast_in_dim.22
  66.6 9.3 %all-to-all-start.3 = ((bf16[8,16,512]{2,1,0:T(8,128)(2,1)}), bf16[8,16,512]{2,1,0:T(8,128)(2,1)S(1)}, u32[]{:S(2)}, u32[]{:S(2)}) async-start(bf16[8,16,512]{2,1,0:T(8,128)(2,1)} %bitcast.30), calls=%async_computation.3 | async-start | bytes 262144 | tf_op jit(solution)/shard_map/all_to_all | solution.py:18
  76.1 5.1 %all-to-all-done.3 = bf16[8,16,512]{2,1,0:T(8,128)(2,1)S(1)} async-done(((bf16[8,16,512]{2,1,0:T(8,128)(2,1)}), bf16[8,16,512]{2,1,0:T(8,128)(2,1)S(1)}, u32[]{:S(2)}, u32[]{:S(2)}) %all-to-all-start.3) | async-done | bytes 131104 | tf_op jit(solution)/shard_map/all_to_all | solution.py:18
  81.2 0.2 reshape.222
  81.6 0.2 reshape.223
  81.8 0.1 fusion.25
  82.0 0.1 fusion.31
  82.3 0.3 convolution_convert_fusion.2
  82.6 1.2 reshape.224
  83.8 6.4 %all-to-all-start.4 = ((bf16[128,2,1024]{2,1,0:T(2,128)(2,1)}), bf16[128,2,1024]{2,1,0:T(2,128)(2,1)S(1)}, u32[]{:S(2)}, u32[]{:S(2)}) async-start(bf16[128,2,1024]{2,1,0:T(2,128)(2,1)} %reshape.224), calls=%async_computation.4 | async-start | bytes 1048576 | tf_op jit(solution)/shard_map/all_to_all | solution.py:18
  90.1 1.5 fusion.59
  91.6 2.3 %convolution_convert_fusion.3 = bf16[16,2048]{1,0:T(8,128)(2,1)S(1)} fusion(bf16[256,2048]{1,0:T(8,128)(2,1)} %param.39, bf16[16,2048]{1,0:T(8,128)(2,1)S(1)} %fusion.33, bf16[2048,256]{1,0:T(8,128)(2,1)} %param.38, f32[16,256]{1,0:T(8,128)S(1)} %fusion.59), kind=kOutput, calls=%fused_computation.9 | convolution fusion | flops 33611776 | bytes 2244608 | tf_op jit(solution)/shard_map/dot_general | solution.py:209
  93.9 4.4 %multiply_add_fusion = f32[16,8,64,64]{3,2,1,0:T(8,128)} fusion(f32[16,8,64,64]{3,2,1,0:T(8,128)} %param.22, f32[16,8,64]{2,1,0:T(8,128)S(1)} %reshape.230, f32[16,8,64]{2,1,0:T(8,128)S(1)} %get-tuple-element.40, f32[8]{0:T(128)S(1)} %dynamic_slice.25), kind=kLoop, calls=%fused_computation.1 | loop fusion | flops 1572864 | bytes 4259872 | tf_op jit(solution)/shard_map/add | solution.py:105
  98.2 10.5 %all-to-all-done.4 = bf16[128,2,1024]{2,1,0:T(2,128)(2,1)S(1)} async-done(((bf16[128,2,1024]{2,1,0:T(2,128)(2,1)}), bf16[128,2,1024]{2,1,0:T(2,128)(2,1)S(1)}, u32[]{:S(2)}, u32[]{:S(2)}) %all-to-all-start.4) | async-done | bytes 524320 | tf_op jit(solution)/shard_map/all_to_all | solution.py:18
  108.8 0.1 copy.42
  108.9 3.1 %collective-permute-start.9 = (bf16[128,2048]{1,0:T(8,128)(2,1)S(1)}, bf16[128,2048]{1,0:T(8,128)(2,1)S(1)}, u32[]{:S(2)}, u32[]{:S(2)}) collective-permute-start(bf16[128,2048]{1,0:T(8,128)(2,1)S(1)} %bitcast.107), channel_id=1, source_target_pairs={{0,1},{1,0},{2,3},{3,2},{4,5},{5,4},{6,7},{7,6},{8,9},{9,8},{10,11... | collective-permute-start | bytes 1572872 | tf_op jit(solution)/shard_map/ppermute | solution.py:26
  112.0 0.3 fusion.15
  112.3 1.5 %fusion.4 = bf16[128,256]{1,0:T(8,128)(2,1)S(1)} fusion(bf16[128,2048]{1,0:T(8,128)(2,1)S(1)} %bitcast.109, bf16[1,2048,256]{2,1,0:T(8,128)(2,1)} %param.35, f32[128,256]{1,0:T(8,128)S(1)} %fusion.15), kind=kOutput, calls=%fused_computation.12 | convolution fusion | flops 134414336 | bytes 1769472 | tf_op jit(solution)/shard_map/dot_general | solution.py:205
  113.9 0.3 fusion.10
  114.2 0.8 convolution_convert_fusion
  115.0 0.1 collective-permute-start.10
  115.2 1.9 %collective-permute-done.10 = bf16[128,2048]{1,0:T(8,128)(2,1)S(1)} collective-permute-done((bf16[128,2048]{1,0:T(8,128)(2,1)S(1)}, bf16[128,2048]{1,0:T(8,128)(2,1)S(1)}, u32[]{:S(2)}, u32[]{:S(2)}) %collective-permute-start.10) | collective-permute-done | bytes 524320 | tf_op jit(solution)/shard_map/ppermute | solution.py:26
  117.0 0.3 fusion.3
  117.4 1.2 reshape.226
  118.5 6.2 %all-to-all-start.5 = ((bf16[128,2,1024]{2,1,0:T(2,128)(2,1)}), bf16[128,2,1024]{2,1,0:T(2,128)(2,1)S(1)}, u32[]{:S(2)}, u32[]{:S(2)}) async-start(bf16[128,2,1024]{2,1,0:T(2,128)(2,1)} %reshape.226), calls=%async_computation.5 | async-start | bytes 1048576 | tf_op jit(solution)/shard_map/all_to_all | solution.py:18
  124.8 19.3 %all-to-all-done.5 = bf16[128,2,1024]{2,1,0:T(2,128)(2,1)S(1)} async-done(((bf16[128,2,1024]{2,1,0:T(2,128)(2,1)}), bf16[128,2,1024]{2,1,0:T(2,128)(2,1)S(1)}, u32[]{:S(2)}, u32[]{:S(2)}) %all-to-all-start.5) | async-done | bytes 524320 | tf_op jit(solution)/shard_map/all_to_all | solution.py:18
  144.1 0.1 copy.43
  144.2 0.2 convolution_add_fusion
  144.4 2.3 %collective-permute-start.11 = (f32[16,2048]{1,0:T(8,128)S(1)}, f32[16,2048]{1,0:T(8,128)S(1)}, u32[]{:S(2)}, u32[]{:S(2)}) collective-permute-start(f32[16,2048]{1,0:T(8,128)S(1)} %convolution_add_fusion), channel_id=1, source_target_pairs={{0,1},{1,0},{2,3},{3,2},{4,5},{5,4},{6,7},{7,6},{8,9},{9,8},{10,11... | collective-permute-start | bytes 393224 | tf_op jit(solution)/shard_map/ppermute | solution.py:26
  146.7 1.0 collective-permute-done.11
  147.7 0.1 multiply_reduce_fusion
  147.9 0.7 fusion.34
  (79 shorter events, 2.1 us)
Async XLA Ops:
  0.6 113.6 %copy-start = (bf16[1,256,2048]{2,1,0:T(8,128)(2,1)S(1)}, bf16[1,256,2048]{2,1,0:T(8,128)(2,1)}, u32[]{:S(2)}) copy-start(bf16[1,256,2048]{2,1,0:T(8,128)(2,1)} %param.36) | copy-start | bytes 3145732
  0.6 45.2 %copy-start.8 = (s32[16]{0:T(128)S(1)}, s32[16]{0:T(128)}, u32[]{:S(2)}) copy-start(s32[16]{0:T(128)} %param.21) | copy-start | bytes 196
  3.1 20.7 %collective-permute-start.2 = (bf16[16,512]{1,0:T(8,128)(2,1)S(1)}, bf16[16,512]{1,0:T(8,128)(2,1)S(1)}, u32[]{:S(2)}, u32[]{:S(2)}) collective-permute-start(bf16[16,512]{1,0:T(8,128)(2,1)S(1)} %get-tuple-element.29), channel_id=1, source_target_pairs={{24,0},{0,8},{8,16},{16,24},{25,1},{1,9},{9,17},{17,25},{26,2},{2,... | collective-permute-start | bytes 49160 | tf_op jit(solution)/shard_map/ppermute | solution.py:36
  5.3 18.4 %collective-permute-start.1 = (bf16[16,512]{1,0:T(8,128)(2,1)S(1)}, bf16[16,512]{1,0:T(8,128)(2,1)S(1)}, u32[]{:S(2)}, u32[]{:S(2)}) collective-permute-start(bf16[16,512]{1,0:T(8,128)(2,1)S(1)} %get-tuple-element.31), channel_id=1, source_target_pairs={{16,0},{24,8},{0,16},{8,24},{17,1},{25,9},{1,17},{9,25},{18,2},{26... | collective-permute-start | bytes 49160 | tf_op jit(solution)/shard_map/ppermute | solution.py:36
  7.9 15.8 %collective-permute-start = (bf16[16,512]{1,0:T(8,128)(2,1)S(1)}, bf16[16,512]{1,0:T(8,128)(2,1)S(1)}, u32[]{:S(2)}, u32[]{:S(2)}) collective-permute-start(bf16[16,512]{1,0:T(8,128)(2,1)S(1)} %get-tuple-element.32), channel_id=1, source_target_pairs={{8,0},{16,8},{24,16},{0,24},{9,1},{17,9},{25,17},{1,25},{10,2},{18... | collective-permute-start | bytes 49160 | tf_op jit(solution)/shard_map/ppermute | solution.py:36
  11.4 28.6 %all-to-all-start = ((bf16[32,16,640]{2,1,0:T(8,128)(2,1)}), bf16[32,16,640]{2,1,0:T(8,128)(2,1)S(1)}, u32[]{:S(2)}, u32[]{:S(2)}) async-start(bf16[32,16,640]{2,1,0:T(8,128)(2,1)} %bitcast.18), calls=%async_computation | async-start | bytes 1310720 | tf_op jit(solution)/shard_map/all_to_all | solution.py:18
  23.9 4.4 %collective-permute-start.3 = (bf16[4,16,512]{2,1,0:T(8,128)(2,1)S(1)}, bf16[4,16,512]{2,1,0:T(8,128)(2,1)S(1)}, u32[]{:S(2)}, u32[]{:S(2)}) collective-permute-start(bf16[4,16,512]{2,1,0:T(8,128)(2,1)S(1)} %get-tuple-element.21), channel_id=1, source_target_pairs={{2,0},{4,2},{6,4},{0,6},{3,1},{5,3},{7,5},{1,7},{10,8},{12,10},{14... | collective-permute-start | bytes 196616 | tf_op jit(solution)/shard_map/ppermute | solution.py:36
  26.4 6.0 %collective-permute-start.5 = (bf16[4,16,512]{2,1,0:T(8,128)(2,1)S(1)}, bf16[4,16,512]{2,1,0:T(8,128)(2,1)S(1)}, u32[]{:S(2)}, u32[]{:S(2)}) collective-permute-start(bf16[4,16,512]{2,1,0:T(8,128)(2,1)S(1)} %get-tuple-element.21), channel_id=1, source_target_pairs={{6,0},{0,2},{2,4},{4,6},{7,1},{1,3},{3,5},{5,7},{14,8},{8,10},{10,... | collective-permute-start | bytes 196616 | tf_op jit(solution)/shard_map/ppermute | solution.py:36
  26.5 5.3 %collective-permute-start.4 = (bf16[4,16,512]{2,1,0:T(8,128)(2,1)S(1)}, bf16[4,16,512]{2,1,0:T(8,128)(2,1)S(1)}, u32[]{:S(2)}, u32[]{:S(2)}) collective-permute-start(bf16[4,16,512]{2,1,0:T(8,128)(2,1)S(1)} %get-tuple-element.21), channel_id=1, source_target_pairs={{4,0},{6,2},{0,4},{2,6},{5,1},{7,3},{1,5},{3,7},{12,8},{14,10},{8,... | collective-permute-start | bytes 196616 | tf_op jit(solution)/shard_map/ppermute | solution.py:36
  41.0 12.4 %all-to-all-start.1 = ((bf16[16,16,512]{2,1,0:T(8,128)(2,1)}), bf16[16,16,512]{2,1,0:T(8,128)(2,1)S(1)}, u32[]{:S(2)}, u32[]{:S(2)}) async-start(bf16[16,16,512]{2,1,0:T(8,128)(2,1)} %bitcast.20), calls=%async_computation.1 | async-start | bytes 524288 | tf_op jit(solution)/shard_map/all_to_all | solution.py:18
  46.1 15.2 %collective-permute-start.8 = (bf16[512,128]{1,0:T(8,128)(2,1)S(1)}, bf16[512,128]{1,0:T(8,128)(2,1)S(1)}, u32[]{:S(2)}, u32[]{:S(2)}) collective-permute-start(bf16[512,128]{1,0:T(8,128)(2,1)S(1)} %slice.29), channel_id=1, source_target_pairs={{6,0},{0,2},{2,4},{4,6},{7,1},{1,3},{3,5},{5,7},{14,8},{8,10},{10,... | collective-permute-start | bytes 393224 | tf_op jit(solution)/shard_map/ppermute | solution.py:36
  47.5 13.8 %collective-permute-start.7 = (bf16[512,128]{1,0:T(8,128)(2,1)S(1)}, bf16[512,128]{1,0:T(8,128)(2,1)S(1)}, u32[]{:S(2)}, u32[]{:S(2)}) collective-permute-start(bf16[512,128]{1,0:T(8,128)(2,1)S(1)} %slice.29), channel_id=1, source_target_pairs={{4,0},{6,2},{0,4},{2,6},{5,1},{7,3},{1,5},{3,7},{12,8},{14,10},{8,... | collective-permute-start | bytes 393224 | tf_op jit(solution)/shard_map/ppermute | solution.py:36
  49.9 11.4 %collective-permute-start.6 = (bf16[512,128]{1,0:T(8,128)(2,1)S(1)}, bf16[512,128]{1,0:T(8,128)(2,1)S(1)}, u32[]{:S(2)}, u32[]{:S(2)}) collective-permute-start(bf16[512,128]{1,0:T(8,128)(2,1)S(1)} %slice.29), channel_id=1, source_target_pairs={{2,0},{4,2},{6,4},{0,6},{3,1},{5,3},{7,5},{1,7},{10,8},{12,10},{14... | collective-permute-start | bytes 393224 | tf_op jit(solution)/shard_map/ppermute | solution.py:36
  53.9 28.0 %copy-start.3 = (bf16[16,2048]{1,0:T(8,128)(2,1)S(1)}, bf16[16,2048]{1,0:T(8,128)(2,1)}, u32[]{:S(2)}) copy-start(bf16[16,2048]{1,0:T(8,128)(2,1)} %param.20) | copy-start | bytes 196612
  53.9 28.0 %copy-start.4 = (f32[2048]{0:T(1024)S(1)}, f32[2048]{0:T(1024)}, u32[]{:S(2)}) copy-start(f32[2048]{0:T(1024)} %param.24) | copy-start | bytes 24580
  53.9 28.2 %copy-start.5 = (f32[2048]{0:T(1024)S(1)}, f32[2048]{0:T(1024)}, u32[]{:S(2)}) copy-start(f32[2048]{0:T(1024)} %param.25) | copy-start | bytes 24580
  57.9 7.7 %all-to-all-start.2 = ((bf16[4,16,512]{2,1,0:T(8,128)(2,1)}), bf16[4,16,512]{2,1,0:T(8,128)(2,1)S(1)}, u32[]{:S(2)}, u32[]{:S(2)}) async-start(bf16[4,16,512]{2,1,0:T(8,128)(2,1)} %broadcast_in_dim.20), calls=%async_computation.2 | async-start | bytes 131072 | tf_op jit(solution)/shard_map/all_to_all | solution.py:18
  66.6 14.6 %all-to-all-start.3 = ((bf16[8,16,512]{2,1,0:T(8,128)(2,1)}), bf16[8,16,512]{2,1,0:T(8,128)(2,1)S(1)}, u32[]{:S(2)}, u32[]{:S(2)}) async-start(bf16[8,16,512]{2,1,0:T(8,128)(2,1)} %bitcast.30), calls=%async_computation.3 | async-start | bytes 262144 | tf_op jit(solution)/shard_map/all_to_all | solution.py:18
  83.8 25.0 %all-to-all-start.4 = ((bf16[128,2,1024]{2,1,0:T(2,128)(2,1)}), bf16[128,2,1024]{2,1,0:T(2,128)(2,1)S(1)}, u32[]{:S(2)}, u32[]{:S(2)}) async-start(bf16[128,2,1024]{2,1,0:T(2,128)(2,1)} %reshape.224), calls=%async_computation.4 | async-start | bytes 1048576 | tf_op jit(solution)/shard_map/all_to_all | solution.py:18
  93.9 18.1 %copy-start.1 = (bf16[1,2048,256]{2,1,0:T(8,128)(2,1)S(1)}, bf16[1,2048,256]{2,1,0:T(8,128)(2,1)}, u32[]{:S(2)}) copy-start(bf16[1,2048,256]{2,1,0:T(8,128)(2,1)} %param.34) | copy-start | bytes 3145732
  108.8 5.1 %copy-start.2 = (bf16[1,2048,256]{2,1,0:T(8,128)(2,1)S(1)}, bf16[1,2048,256]{2,1,0:T(8,128)(2,1)}, u32[]{:S(2)}) copy-start(bf16[1,2048,256]{2,1,0:T(8,128)(2,1)} %param.35) | copy-start | bytes 3145732
  108.9 5.0 %collective-permute-start.9 = (bf16[128,2048]{1,0:T(8,128)(2,1)S(1)}, bf16[128,2048]{1,0:T(8,128)(2,1)S(1)}, u32[]{:S(2)}, u32[]{:S(2)}) collective-permute-start(bf16[128,2048]{1,0:T(8,128)(2,1)S(1)} %bitcast.107), channel_id=1, source_target_pairs={{0,1},{1,0},{2,3},{3,2},{4,5},{5,4},{6,7},{7,6},{8,9},{9,8},{10,11... | collective-permute-start | bytes 1572872 | tf_op jit(solution)/shard_map/ppermute | solution.py:26
  114.2 10.5 %copy-start.7 = (f32[16,6]{0,1:T(8,128)S(1)}, f32[16,6]{0,1:T(8,128)}, u32[]{:S(2)}) copy-start(f32[16,6]{0,1:T(8,128)} %param.33) | copy-start | bytes 1156
  114.2 33.6 %copy-start.6 = (f32[2048]{0:T(1024)S(1)}, f32[2048]{0:T(1024)}, u32[]{:S(2)}) copy-start(f32[2048]{0:T(1024)} %param.26) | copy-start | bytes 24580
  115.0 2.0 %collective-permute-start.10 = (bf16[128,2048]{1,0:T(8,128)(2,1)S(1)}, bf16[128,2048]{1,0:T(8,128)(2,1)S(1)}, u32[]{:S(2)}, u32[]{:S(2)}) collective-permute-start(bf16[128,2048]{1,0:T(8,128)(2,1)S(1)} %convolution_convert_fusion), channel_id=1, source_target_pairs={{0,1},{1,0},{2,3},{3,2},{4,5},{5,4},{6,7},{7,6},{8,9},{9,8},{10,11... | collective-permute-start | bytes 1572872 | tf_op jit(solution)/shard_map/ppermute | solution.py:26
  118.5 25.6 %all-to-all-start.5 = ((bf16[128,2,1024]{2,1,0:T(2,128)(2,1)}), bf16[128,2,1024]{2,1,0:T(2,128)(2,1)S(1)}, u32[]{:S(2)}, u32[]{:S(2)}) async-start(bf16[128,2,1024]{2,1,0:T(2,128)(2,1)} %reshape.226), calls=%async_computation.5 | async-start | bytes 1048576 | tf_op jit(solution)/shard_map/all_to_all | solution.py:18
  144.4 3.3 %collective-permute-start.11 = (f32[16,2048]{1,0:T(8,128)S(1)}, f32[16,2048]{1,0:T(8,128)S(1)}, u32[]{:S(2)}, u32[]{:S(2)}) collective-permute-start(f32[16,2048]{1,0:T(8,128)S(1)} %convolution_add_fusion), channel_id=1, source_target_pairs={{0,1},{1,0},{2,3},{3,2},{4,5},{5,4},{6,7},{7,6},{8,9},{9,8},{10,11... | collective-permute-start | bytes 393224 | tf_op jit(solution)/shard_map/ppermute | solution.py:26
